TPU v7x, 128 devices: a whole 4x4x4 slice. The times are simulated.
128 devices in a mesh: fs: 16 (over z, x), tp: 8 (over y, core).
Axes of the slice: x: 4, y: 4, z: 4, core: 2. Of those that a mesh axis runs over, the one named last changes fastest.
Arguments:
- saved_input: bfloat16 [49152, 2048], P('fs'), may hold values from -6 to 6
- proj_cot: bfloat16 [3, 49152, 2048], P(None, 'fs', 'tp'), may hold values from -0.02734375 to 0.02734375
- log_cache: float32 [16, 49152], P(None, 'fs'), as said below
- cache_cot: float32 [16, 49152], P(None, 'fs'), may hold values from -0.02734375 to 0.02734375
- proj_master: float32 [3, 2048, 2048], P(None, 'fs', 'tp'), may hold values from -0.125 to 0.125
- factors: bfloat16 [3, 2048, 256], P(None, 'fs'), may hold values from -0.125 to 0.125
- first_moment: float32 [3, 256, 2048], P(None, None, 'tp'), may hold values from -6 to 6
- second_moment: float32 [3, 256, 2048], P(None, None, 'tp'), may hold values from 0.01 to 10
- gate_master: float32 [16, 2048], replicated, may hold values from -0.125 to 0.125
- gate_first: float32 [16, 2048], replicated, may hold values from -6 to 6
- gate_second: float32 [16, 2048], replicated, may hold values from 0.1 to 3
Outputs:
- proj_step: float32 [3, 2048, 2048], P(None, 'fs', 'tp')
- proj_new: float32 [3, 2048, 2048], P(None, 'fs', 'tp')
- proj_copy: bfloat16 [3, 2048, 2048], P(None, None, 'tp')
- first_new: float32 [3, 256, 2048], P(None, None, 'tp')
- second_new: float32 [3, 256, 2048], P(None, None, 'tp')
- gate_new: float32 [16, 2048], replicated
- gate_copy: bfloat16 [16, 2048], replicated
- gate_first_new: float32 [16, 2048], replicated
- gate_second_new: float32 [16, 2048], replicated
Inputs may be any that keep to these rules, and one draw needn't show every extreme that they name: `log_cache`: each head's values never rise along positions.
All inputs are finite; a program needn't handle non-finite values.
Results may differ from a plain program's by a relative error of at most 0.0004.
Values may be sent and summed in bfloat16 or wider, within the bound.
A program may use at most 128 MiB of HBM per device.

v0:
```python
import jax
import jax.numpy as jnp
from jax import lax
from jax.sharding import PartitionSpec as P

BETA_ONE = 0.8
BETA_TWO = 0.9
LEARN = 0.001


def from_behind(x, axis, by):
    peers = lax.axis_size(axis)
    pairs = [(i, i + by) for i in range(peers) if 0 <= i + by < peers]
    return lax.ppermute(x, axis, pairs)


def from_everyone(x, axis):
    copies = jnp.broadcast_to(x, (lax.axis_size(axis), *x.shape))
    return lax.all_to_all(copies, axis, split_axis=0, concat_axis=0, tiled=True)


def folded_in_pairs(pieces, combine):
    while len(jax.tree.leaves(pieces)[0]) > 1:
        pieces = jax.vmap(combine)(*(pieces[side::2] for side in (0, 1)))
    return pieces[0]


def carried_in(x, axis, combine, identity):
    peers, place = (lax.axis_size(axis), lax.axis_index(axis))
    passed = jnp.arange(peers) > place

    def kept(part, zero, own):
        part = jnp.where(
            passed.reshape(-1, *(1 for _ in own.shape)), part, jnp.asarray(zero, own.dtype)
        )
        return part[::-1]

    pieces = from_everyone(x, axis)
    return folded_in_pairs(kept(pieces, identity, x), combine)


def rows_for(lines, peers):
    spare = -lines.shape[0] % peers
    if not spare:
        return lines
    return jnp.concatenate([lines, jnp.zeros((spare, *lines.shape[1:]), lines.dtype)])


def in_order(parts, dim):
    parts = jnp.moveaxis(parts, 0, dim)
    lengths = parts.shape
    return parts.reshape(*lengths[:dim], lengths[dim] * lengths[dim + 1], *lengths[dim + 2 :])


def collect(x, axis, dim):
    return in_order(from_everyone(x, axis), dim)


def cut_along(x, dim, peers):
    lengths = x.shape
    parts = x.reshape(*lengths[:dim], peers, lengths[dim] // peers, *lengths[dim + 1 :])
    return jnp.moveaxis(parts, dim, 0)


def summed_on_arrival(x, axis, dim):
    parts = cut_along(x, dim, lax.axis_size(axis))
    arrived = lax.all_to_all(parts, axis, split_axis=0, concat_axis=0, tiled=True)
    return arrived.sum(axis=0)


def total_of(x, axes):
    padded = rows_for(x, lax.axis_size(axes))
    whole = collect(summed_on_arrival(padded, axes, 0), axes, 0)
    return lax.slice_in_dim(whole, 0, len(x)).reshape(x.shape)


def in_one(arrays, axis):
    ravelled, at, finished = (jnp.concatenate([a.reshape(-1) for a in arrays]), 0, [])
    so_far = total_of(ravelled, axis)
    for a in arrays:
        finished.append(so_far[at : at + a.size].reshape(a.shape))
        at += a.size
    return tuple(finished)


def over_copies(x, axis):
    everything = from_everyone(x, axis)
    return jnp.sum(everything, axis=0)


def add_pair(earlier, later_part):
    return earlier + later_part


def local(
    saved_input,
    proj_cot,
    log_cache,
    cache_cot,
    proj_master,
    factors,
    first_moment,
    second_moment,
    gate_master,
    gate_first,
    gate_second,
):
    heads = log_cache.shape[0]
    edge = from_behind(log_cache[:, -1:], "fs", 1)
    previous = jnp.concatenate([edge, log_cache[:, :-1]], axis=1)
    gate_logarithm = log_cache - previous
    carried = carried_in(
        jnp.sum(cache_cot, axis=1), "fs", add_pair, jnp.zeros((heads,), jnp.float32)
    )
    later = jnp.flip(jnp.cumsum(jnp.flip(cache_cot, 1), axis=1), 1) + carried[:, None]
    gate_cot = (later * -jnp.expm1(gate_logarithm)).astype(jnp.bfloat16)
    gate_part = jnp.dot(gate_cot, saved_input, preferred_element_type=jnp.float32)
    all_factors = lax.all_gather(factors, "fs", axis=1, tiled=True)
    reduced = jnp.einsum(
        "td,rdk->rtk", saved_input, all_factors, preferred_element_type=jnp.float32
    )
    upper_half = lax.optimization_barrier(reduced.astype(jnp.bfloat16))
    lower_half = (reduced - upper_half.astype(jnp.float32)).astype(jnp.bfloat16)
    low_part = jnp.einsum("rtk,rtw->rkw", upper_half, proj_cot, preferred_element_type=jnp.float32)
    low_part = low_part + jnp.einsum(
        "rtk,rtw->rkw", lower_half, proj_cot, preferred_element_type=jnp.float32
    )
    low, gate_grad = in_one((low_part, gate_part), "fs")
    first_new = BETA_ONE * first_moment + (1.0 - BETA_ONE) * low
    second_new = BETA_TWO * second_moment + (1.0 - BETA_TWO) * low * low
    direction = first_new / jnp.sqrt(second_new)
    squares = over_copies(jnp.sum(direction * direction), "tp")
    entries = direction.shape[0] * direction.shape[1] * direction.shape[2] * lax.axis_size("tp")
    scale = lax.rsqrt(squares / entries + 1e-06)
    product = jnp.einsum(
        "rdk,rkw->rdw", factors.astype(jnp.float32), direction, precision=lax.Precision.HIGHEST
    )
    proj_step = scale * product
    proj_new = proj_master - LEARN * proj_step
    proj_copy = lax.all_gather(proj_new.astype(jnp.bfloat16), "fs", axis=1, tiled=True)
    gate_first_new = BETA_ONE * gate_first + (1.0 - BETA_ONE) * gate_grad
    gate_second_new = BETA_TWO * gate_second + (1.0 - BETA_TWO) * gate_grad * gate_grad
    gate_new = gate_master - LEARN * gate_first_new / jnp.sqrt(gate_second_new)
    gate_copy = gate_new.astype(jnp.bfloat16)
    return (
        proj_step,
        proj_new,
        proj_copy,
        first_new,
        second_new,
        gate_new,
        gate_copy,
        gate_first_new,
        gate_second_new,
    )


def solution(mesh):
    placed = (
        P("fs", None),
        P(None, "fs", "tp"),
        P(None, "fs"),
        P(None, "fs"),
        P(None, "fs", "tp"),
        P(None, "fs", None),
        P(None, None, "tp"),
        P(None, None, "tp"),
        P(),
        P(),
        P(),
    )
    return jax.shard_map(
        local,
        mesh=mesh,
        in_specs=placed,
        out_specs=(
            P(None, "fs", "tp"),
            P(None, "fs", "tp"),
            P(None, None, "tp"),
            P(None, None, "tp"),
            P(None, None, "tp"),
            P(),
            P(),
            P(),
            P(),
        ),
        check_vma=False,
    )
```

profile of v0, /device:TPU:0, one launch (start us, length us, event | category | flops | bytes accessed | tf_op | source)
XLA Modules:
  0.0 206.4 jit_solution(16304343146461172091)
XLA Ops:
  7.2 0.0 all-gather.3.cloned.1.call-start
  7.2 1.7 copy.44
  9.0 0.0 all-gather.3.cloned.1.call-update
  9.0 1.1 reduce_sum.36
  10.1 0.6 broadcast_in_dim.22
  10.7 8.0 %all-to-all-start = ((f32[16,1,16]{2,1,0:T(1,128)}), f32[16,1,16]{2,1,0:T(1,128)S(1)}, u32[]{:S(2)}, u32[]{:S(2)}) async-start(f32[16,1,16]{2,1,0:T(1,128)} %broadcast_in_dim.22), calls=%async_computation | async-start | bytes 16384 | tf_op jit(solution)/shard_map/all_to_all | solution.py:19
  18.7 0.8 slice.65
  19.4 3.8 %collective-permute-start = (f32[16,1]{1,0:T(8,128)S(1)}, f32[16,1]{1,0:T(8,128)S(1)}, u32[]{:S(2)}, u32[]{:S(2)}) collective-permute-start(f32[16,1]{1,0:T(8,128)S(1)} %slice.65), channel_id=1, source_target_pairs={{0,8},{8,16},{16,24},{24,32},{32,40},{40,48},{48,56},{56,64},{64,7... | collective-permute-start | bytes 200 | tf_op jit(solution)/shard_map/ppermute | solution.py:14
  23.3 9.3 %rev.8 = f32[16,3072]{1,0:T(8,128)S(1)} reverse(f32[16,3072]{1,0:T(8,128)} %param.14), dimensions={1} | reverse | bytes 393216 | tf_op jit(solution)/shard_map/jit(_flip)/rev | solution.py:115
  32.6 4.6 %reduce-window.6 = f32[16,24,128]{2,1,0:T(8,128)S(1)} reduce-window(f32[16,24,128]{2,1,0:T(8,128)S(1)} %bitcast.46, f32[]{:T(128)} %constant.11.clone.1), window={size=1x1x128 pad=0_0x0_0x127_0}, to_apply=%region_0.0 | reduce-window | flops 6242304 | bytes 393220 | tf_op jit(solution)/shard_map/reduce-window
  37.3 0.2 slice_reduce_fusion
  37.5 0.2 reduce-window.9
  37.7 0.1 broadcast_add_fusion
  37.8 1.8 rev.9
  39.6 0.0 all-to-all-done
  39.6 0.1 broadcast_select_fusion
  39.9 0.0 collective-permute-done
  39.9 6.6 %convolution_bitcast_fusion = f32[2,16,8,128]{3,2,1,0:T(8,128)S(1)} fusion(bf16[3072,2048]{1,0:T(8,128)(2,1)} %param.11, f32[16,3072]{1,0:T(8,128)} %param.13, f32[16,3071]{1,0:T(8,128)} %bitcast.43, f32[16,1]{1,0:T(8,128)S(1)} %collective-permute-done, f32[16,3072]{1,0:T(8,128)S(1)} %rev.9, f32[16]{0:T(128)S(1)} %add_bitcast_fusion), kind=kOutput, calls=%fused_computation.10 | convolution fusion | flops 201621504 | bytes 13303872 | tf_op jit(solution)/shard_map/dot_general | solution.py:117
  46.5 18.7 %all-gather.3.cloned.1.call-done = bf16[3,2048,256]{1,2,0:T(8,128)(2,1)} async-done(((bf16[3,128,256]{1,2,0:T(8,128)(2,1)}), bf16[3,2048,256]{1,2,0:T(8,128)(2,1)}) %all-gather.3.cloned.1.call-update) | async-done | bytes 3145744 | tf_op jit(solution)/shard_map/all_gather | solution.py:118
  65.3 16.1 %bitcast_convert_fusion = (bf16[3,3072,256]{1,2,0:T(8,128)(2,1)S(1)}, f32[3,256,3072]{2,1,0:T(8,128)}) fusion(bf16[3,2048,256]{1,2,0:T(8,128)(2,1)} %all-gather.3.cloned.1.call-done, bf16[3072,2048]{1,0:T(8,128)(2,1)} %param.11), kind=kOutput, calls=%fused_computation.3 | convolution fusion | flops 9666035712 | bytes 29884416 | tf_op jit(solution)/shard_map/td,rdk->rtk/dot_general | solution.py:119
  81.4 3.7 %fusion.22 = f32[3,256,256]{2,1,0:T(8,128)S(1)} fusion(bf16[3,3072,256]{1,2,0:T(8,128)(2,1)S(1)} %get-tuple-element.63, bf16[3,3072,256]{2,1,0:T(8,128)(2,1)} %param.12), kind=kOutput, calls=%fused_computation.36 | convolution fusion | flops 1207959552 | bytes 10223616 | tf_op jit(solution)/shard_map/rtk,rtw->rkw/dot_general | solution.py:124
  85.1 6.4 %fusion.5 = f32[3,256,256]{2,1,0:T(8,128)S(1)} fusion(f32[3,256,256]{2,1,0:T(8,128)S(1)} %fusion.22, bf16[3,3072,256]{2,1,0:T(8,128)(2,1)} %param.12, f32[3,256,3072]{2,1,0:T(8,128)} %get-tuple-element.64, bf16[3,3072,256]{1,2,0:T(8,128)(2,1)S(1)} %get-tuple-element.63), kind=kOutput, calls=%fused_computation.6 | convolution fusion | flops 1215234048 | bytes 20447232 | tf_op jit(solution)/shard_map/rtk,rtw->rkw/dot_general | solution.py:125
  91.5 0.0 copy-start.3
  91.5 0.4 copy.55
  91.9 0.1 pad_maximum_fusion
  92.0 19.2 %all_to_all.30 = f32[16,1,14336]{2,1,0:T(1,128)S(1)} all-to-all(f32[16,1,14336]{2,1,0:T(1,128)S(1)} %bitcast.40), channel_id=1, replica_groups=mesh['fs'=16,'tp'=8] {'fs'}, dimensions={0} | all-to-all | bytes 1835008 | tf_op jit(solution)/shard_map/all_to_all | solution.py:67
  111.2 0.6 reduce_sum.37
  111.8 1.4 broadcast_in_dim.24
  113.2 0.0 copy-start.2
  113.2 3.8 %all-to-all-start.2 = ((f32[16,1,14336]{2,1,0:T(1,128)}), f32[16,1,14336]{2,1,0:T(1,128)S(1)}, u32[]{:S(2)}, u32[]{:S(2)}) async-start(f32[16,1,14336]{2,1,0:T(1,128)} %broadcast_in_dim.24), calls=%async_computation.2 | async-start | bytes 1835008 | tf_op jit(solution)/shard_map/all_to_all | solution.py:19
  117.0 0.2 all-gather.5.cloned.1.call-start
  117.2 0.0 copy-done.3
  117.2 0.9 copy.48
  118.1 12.4 %all-to-all-done.2 = f32[16,1,14336]{2,1,0:T(1,128)S(1)} async-done(((f32[16,1,14336]{2,1,0:T(1,128)}), f32[16,1,14336]{2,1,0:T(1,128)S(1)}, u32[]{:S(2)}, u32[]{:S(2)}) %all-to-all-start.2) | async-done | bytes 917536 | tf_op jit(solution)/shard_map/all_to_all | solution.py:19
  130.5 0.1 slice.72
  130.6 0.2 reshape.69
  130.8 2.3 %multiply_reduce_fusion = (f32[]{:T(128)}, f32[3,256,256]{2,1,0:T(8,128)S(1)}, f32[3,256,256]{2,1,0:T(8,128)S(1)}) fusion(f32[3,256,256]{2,1,0:T(8,128)S(1)} %reshape.69, f32[3,256,256]{2,1,0:T(8,128)} %param.18, f32[3,256,256]{2,1,0:T(8,128)} %param.17), kind=kLoop, calls=%fused_computation.13 | loop fusion | flops 1966079 | bytes 3932164 | tf_op jit(solution)/shard_map/reduce_sum | solution.py:132
  133.1 0.0 copy-start.1
  133.1 0.0 copy-start
  133.1 0.0 copy-start.4
  133.1 0.0 copy-start.5
  133.1 0.7 broadcast_in_dim.25
  133.8 9.4 %all_to_all.31 = f32[8,1,1]{2,1,0:T(1,128)S(1)} all-to-all(f32[8,1,1]{2,1,0:T(1,128)S(1)} %broadcast_in_dim.25), channel_id=1, replica_groups=mesh['fs'=16,'tp'=8] {'tp'}, dimensions={0} | all-to-all | bytes 64 | tf_op jit(solution)/shard_map/all_to_all | solution.py:19
  143.2 0.6 reduce_sum.39
  144.5 0.0 copy-done.2
  144.5 2.7 %fusion.20 = (bf16[3,128,256]{1,2,0:T(8,128)(2,1)}, f32[3,128,256]{1,2,0:T(8,128)S(1)}, f32[3,128,256]{1,2,0:T(8,128)}) fusion(f32[3,128,256]{1,2,0:T(8,128)} %copy.48, bf16[3,128,256]{2,1,0:T(8,128)(2,1)S(1)} %copy-done.2, f32[3,256,256]{2,1,0:T(8,128)S(1)} %get-tuple-element.62, f32[3,256,256]{2,1,0:T(8,128)S(1)} %get-tuple-element.61, f32[]{:T(128)S(6)} %rsqrt.5), kind=kOutput, calls=%fused_computation.35 | convolution fusion | flops 302579712 | bytes 3145732 | tf_op jit(solution)/shard_map/rdk,rkw->rdw/dot_general | solution.py:135
  147.1 0.0 copy-done.1
  147.1 0.0 all-gather.5.cloned.1.call-update
  147.2 2.2 %reduce.3 = f32[16,14336]{1,0:T(8,128)S(1)} reduce(f32[16,1,14336]{2,1,0:T(1,128)S(1)} %all-to-all-done.2, f32[]{:T(128)} %constant.8), dimensions={1}, to_apply=%all_to_all.24.reduce_sub_computation | reduce | bytes 1835012 | tf_op jit(solution)/shard_map/all_to_all | solution.py:19
  149.4 0.1 slice.68
  149.5 0.0 copy-done.4
  149.5 0.0 copy-done.5
  149.5 1.7 fusion.18
  151.2 1.9 copy.49
  153.1 0.9 copy.50
  154.1 0.0 copy-done
  154.1 40.8 %all-gather.5.cloned.1.call-done = bf16[3,2048,256]{1,2,0:T(8,128)(2,1)} async-done(((bf16[3,128,256]{1,2,0:T(8,128)(2,1)}), bf16[3,2048,256]{1,2,0:T(8,128)(2,1)}) %all-gather.5.cloned.1.call-update) | async-done | bytes 3145744 | tf_op jit(solution)/shard_map/all_gather | solution.py:140
  194.9 4.6 %copy.51 = bf16[3,2048,256]{2,1,0:T(8,128)(2,1)} copy(bf16[3,2048,256]{1,2,0:T(8,128)(2,1)} %all-gather.5.cloned.1.call-done) | data formatting | bytes 6291456
  (16 shorter events, 0.3 us)
Async XLA Ops:
  7.2 58.1 %all-gather.3.cloned.1.call-start = ((), (), s32[]{:S(2)}) async-start(), calls=%async_computation.4 | async-start | bytes 3342336 | tf_op jit(solution)/shard_map/all_gather | solution.py:118
  10.7 28.9 %all-to-all-start = ((f32[16,1,16]{2,1,0:T(1,128)}), f32[16,1,16]{2,1,0:T(1,128)S(1)}, u32[]{:S(2)}, u32[]{:S(2)}) async-start(f32[16,1,16]{2,1,0:T(1,128)} %broadcast_in_dim.22), calls=%async_computation | async-start | bytes 16384 | tf_op jit(solution)/shard_map/all_to_all | solution.py:19
  19.4 20.4 %collective-permute-start = (f32[16,1]{1,0:T(8,128)S(1)}, f32[16,1]{1,0:T(8,128)S(1)}, u32[]{:S(2)}, u32[]{:S(2)}) collective-permute-start(f32[16,1]{1,0:T(8,128)S(1)} %slice.65), channel_id=1, source_target_pairs={{0,8},{8,16},{16,24},{24,32},{32,40},{40,48},{48,56},{56,64},{64,7... | collective-permute-start | bytes 200 | tf_op jit(solution)/shard_map/ppermute | solution.py:14
  91.5 25.7 %copy-start.3 = (f32[3,128,256]{2,1,0:T(8,128)S(1)}, f32[3,128,256]{2,1,0:T(8,128)}, u32[]{:S(2)}) copy-start(f32[3,128,256]{2,1,0:T(8,128)} %param.15) | copy-start | bytes 1179652
  113.2 31.3 %copy-start.2 = (bf16[3,128,256]{2,1,0:T(8,128)(2,1)S(1)}, bf16[3,128,256]{2,1,0:T(8,128)(2,1)}, u32[]{:S(2)}) copy-start(bf16[3,128,256]{2,1,0:T(8,128)(2,1)} %param.16) | copy-start | bytes 589828
  113.2 17.3 %all-to-all-start.2 = ((f32[16,1,14336]{2,1,0:T(1,128)}), f32[16,1,14336]{2,1,0:T(1,128)S(1)}, u32[]{:S(2)}, u32[]{:S(2)}) async-start(f32[16,1,14336]{2,1,0:T(1,128)} %broadcast_in_dim.24), calls=%async_computation.2 | async-start | bytes 1835008 | tf_op jit(solution)/shard_map/all_to_all | solution.py:19
  117.0 77.9 %all-gather.5.cloned.1.call-start = ((), (), s32[]{:S(2)}) async-start(), calls=%async_computation.5 | async-start | bytes 3342336 | tf_op jit(solution)/shard_map/all_gather | solution.py:140
  133.1 14.1 %copy-start.1 = (f32[3,256,256]{2,1,0:T(8,128)}, f32[3,256,256]{2,1,0:T(8,128)S(1)}, u32[]{:S(2)}) copy-start(f32[3,256,256]{2,1,0:T(8,128)S(1)} %get-tuple-element.62) | copy-start | bytes 2359300
  133.1 21.0 %copy-start = (f32[3,256,256]{2,1,0:T(8,128)}, f32[3,256,256]{2,1,0:T(8,128)S(1)}, u32[]{:S(2)}) copy-start(f32[3,256,256]{2,1,0:T(8,128)S(1)} %get-tuple-element.61) | copy-start | bytes 2359300
  133.1 16.5 %copy-start.4 = (f32[16,2048]{1,0:T(8,128)S(1)}, f32[16,2048]{1,0:T(8,128)}, u32[]{:S(2)}) copy-start(f32[16,2048]{1,0:T(8,128)} %param.19) | copy-start | bytes 393220
  133.1 16.5 %copy-start.5 = (f32[16,2048]{1,0:T(8,128)S(1)}, f32[16,2048]{1,0:T(8,128)}, u32[]{:S(2)}) copy-start(f32[16,2048]{1,0:T(8,128)} %param.20) | copy-start | bytes 393220
Sparse Core Ops, SparseCore 0:
  10.7 54.5 all-gather.2
  147.3 47.5 all-gather.4
where the time goes:
time: 208 us; the launch traced here: 206 us
  waiting for transfers between devices  72 us (35%)
  matrix products  35.5 us (17%)
  blocking collectives  28.6 us (14%)
  local copies, waits for them, and re-layouts  26.1 us (13%)
  starting transfers between devices  15.8 us (8%)
  between operations  14.9 us (7%)
  other arithmetic  13.5 us (6%)
    all_gather x1, waiting for transfers between devices, local(): lax.all_gather(proj_new.astype(jnp.bfloat16), 'fs', axis=1, tiled=True)  40.8 us
    all_to_all x1, blocking collectives, summed_on_arrival(): lax.all_to_all(parts, axis, split_axis=0, concat_axis=0, tiled=True)  19.2 us
    all_gather x1, waiting for transfers between devices, local(): all_factors = lax.all_gather(factors, 'fs', axis=1, tiled=True)  18.7 us
    dot_general x1, matrix products, local(): jnp.einsum('td,rdk->rtk', saved_input, all_factors, preferred_element_typ...  16.1 us
    all_to_all x2, waiting for transfers between devices, from_everyone(): return lax.all_to_all(copies, axis, split_axis=0, concat_axis=0, tiled=True)  12.4 us
    all_to_all x2, starting transfers between devices, from_everyone(): return lax.all_to_all(copies, axis, split_axis=0, concat_axis=0, tiled=True)  11.8 us
    unnamed x21, local copies, waits for them, and re-layouts  10.7 us
    all_to_all x1, blocking collectives, from_everyone(): return lax.all_to_all(copies, axis, split_axis=0, concat_axis=0, tiled=True)  9.37 us
  transfers between devices with their start and end apart: 5, of which 3 were waited for; matrix products, arithmetic and copies ran while one was open for 16% of the time, Pallas kernels for 0%

commit v1 on v0

v1 whole, which is shorter than its diff:
```python
import functools

import jax
import jax.numpy as jnp
from jax import lax
from jax.experimental import pallas as pl
from jax.experimental.pallas import tpu as pltpu
from jax.sharding import PartitionSpec as P

BETA_ONE = 0.8
BETA_TWO = 0.9
LEARN = 0.001
MESH = pl.DeviceIdType.MESH
F32, BF16 = jnp.float32, jnp.bfloat16

FS, TP, RING = 16, 8, 4
ROLES, TOK, DIM, COLS, RANK, HEADS = 3, 3072, 2048, 256, 256, 16
BLOCK = 512
BLOCKS = DIM // BLOCK
SLICE = RANK // FS
TURN = TOK // BLOCKS


def minus_expm1(x):
    series = jnp.ones_like(x)
    for n in range(9, 1, -1):
        series = 1.0 + x * (1.0 / n) * series
    return jnp.where(jnp.abs(x) < 0.5, -x * series, 1.0 - jnp.exp(x))


def halves(x):
    upper = x.astype(BF16)
    return upper, (x - upper.astype(F32)).astype(BF16)


class Gather:
    def __init__(self, me, piece, send, recv):
        self.me, self.piece, self.send, self.recv = me, piece, send, recv
        x, z = me % RING, me // RING
        self.at = ((x, z), (z, x))

    def name(self, half, first, second):
        return second * RING + first if half == 0 else first * RING + second

    def copy(self, half, index):
        p, q = self.at[half]
        turn = lambda a, b: (a + b + RING) % RING
        if index < 3:
            d = index + 1
            out, to = (p, q), (turn(p, d), q)
            came = (turn(p, -d), q)
        else:
            e, kind = divmod(index - 3, 3)
            first = turn(p, -e)
            up = e < 2
            if kind == 0:
                out, to, came = (first, q), (p, turn(q, 1)), (first, turn(q, -1))
            elif kind == 1:
                out, to, came = (first, q), (p, turn(q, -1)), (first, turn(q, 1))
            elif up:
                out, to, came = (first, turn(q, -1)), (p, turn(q, 1)), (first, turn(q, 2))
            else:
                out, to, came = (first, turn(q, 1)), (p, turn(q, -1)), (first, turn(q, 2))
        return self.name(half, *out), self.name(half, *to), self.name(half, *came)

    def start(self, half, index):
        out, to, _ = self.copy(half, index)
        ref = self.piece(out, half)
        pltpu.make_async_remote_copy(
            ref, ref, self.send.at[half, index], self.recv.at[half, index], device_id={"fs": to}, device_id_type=MESH
        ).start()

    def waiter(self, half, index, sent):
        out, to, came = self.copy(half, index)
        ref = self.piece(out if sent else came, half)
        return pltpu.make_async_remote_copy(
            ref, ref, self.send.at[half, index], self.recv.at[half, index], device_id={"fs": to}, device_id_type=MESH
        )

    def arrived(self, half, index):
        self.waiter(half, index, False).wait_recv()

    def first(self):
        for index in (0, 1, 2, 3, 4):
            for half in (0, 1):
                self.start(half, index)

    def second(self):
        for half in (0, 1):
            self.arrived(half, 3)
            self.start(half, 5)
        for e in (1, 3, 2):
            for half in (0, 1):
                self.arrived(half, e - 1)
                self.start(half, 3 + 3 * e)
                self.start(half, 4 + 3 * e)

    def third(self):
        for e in (1, 3, 2):
            for half in (0, 1):
                self.arrived(half, 3 + 3 * e if e < 2 else 4 + 3 * e)
                self.start(half, 5 + 3 * e)

    def last(self):
        for half in (0, 1):
            for e in range(4):
                self.arrived(half, 4 + 3 * e if e < 2 else 3 + 3 * e)
                self.arrived(half, 5 + 3 * e)

    def drain(self):
        for half in (0, 1):
            for index in range(15):
                self.waiter(half, index, True).wait_send()


def kernel(
    x_hbm, cot_hbm, logs_hbm, ccot_hbm, master_hbm, factors_hbm, first_hbm, second_hbm, gm_hbm, gf_hbm, gs_hbm,
    step_ref, new_ref, copy_ref, first_ref, second_ref, gnew_ref, gcopy_ref, gfirst_ref, gsecond_ref,
    x_v, cot_v, logs_v, ccot_v, master_v, fac_v, fm_v, sm_v, gm_v, gf_v, gs_v,
    lhs_v, grad_v, later_v, gate_v, gx_v, lowp_v, rs_v, low_v, gp_v, grs_v, gfull_v, prod_v, sum_v, ss_v,
    in_sem, x_sem, cot_sem, gx_send, gx_recv, rs_send, rs_recv, ag_send, ag_recv, gr_send, gr_recv, ga_send, ga_recv,
    ss_send, ss_recv, f_send, f_recv, d_send, d_recv, c_send, c_recv,
):
    me, tp = lax.axis_index("fs"), lax.axis_index("tp")
    core = tp % 2

    def load(src, dst, sem):
        return pltpu.make_async_copy(src, dst, sem)

    fac_in = [
        load(factors_hbm.at[:, pl.ds(pl.multiple_of(64 * h + 32 * core, 32), 32), :], fac_v.at[:, 2 * me + h, core], in_sem.at[h])
        for h in (0, 1)
    ]
    logs_in = load(logs_hbm, logs_v, in_sem.at[2])
    ccot_in = load(ccot_hbm, ccot_v, in_sem.at[3])
    cot_in = [load(cot_hbm.at[r], cot_v.at[r], cot_sem.at[r]) for r in range(ROLES)]
    x_in = [load(x_hbm.at[:, pl.ds(BLOCK * n, BLOCK)], x_v.at[n], x_sem.at[n]) for n in range(BLOCKS)]
    rest_in = [
        load(s, d, in_sem.at[4 + i])
        for i, (s, d) in enumerate(
            ((first_hbm, fm_v), (second_hbm, sm_v), (master_hbm, master_v), (gm_hbm, gm_v), (gf_hbm, gf_v), (gs_hbm, gs_v))
        )
    ]
    for c in (*fac_in, ccot_in, logs_in, cot_in[0], *x_in, cot_in[1], cot_in[2], *rest_in):
        c.start()

    barrier = pltpu.get_barrier_semaphore()

    @pl.loop(1, FS)
    def _(d):
        pl.semaphore_signal(barrier, inc=1, device_id={"fs": (me + d) % FS}, device_id_type=MESH)

    @pl.loop(1, TP)
    def _(d):
        pl.semaphore_signal(barrier, inc=1, device_id={"tp": (tp + d) % TP}, device_id_type=MESH)

    ccot_in.wait()
    lane = lax.broadcasted_iota(jnp.int32, (HEADS, TOK), 1)
    later = ccot_v[...]
    by = 1
    while by < TOK:
        later = later + jnp.where(lane < TOK - by, pltpu.roll(later, TOK - by, 1), 0.0)
        by *= 2
    later_v[...] = later
    logs_in.wait()
    logs = logs_v[...]
    gate_v[...] = minus_expm1(logs - pltpu.roll(logs, 1, 1))
    small = lax.broadcasted_iota(jnp.int32, (HEADS, 128), 1)
    gx_v[me] = jnp.where(
        small < 64,
        jnp.broadcast_to(later[:, 0:1], (HEADS, 128)),
        jnp.broadcast_to(logs[:, TOK - 1 : TOK], (HEADS, 128)),
    )

    pl.semaphore_wait(barrier, FS + TP - 2)

    def to_peers(src, dst, send, recv, sem):
        @pl.loop(1, FS)
        def _(d):
            peer = (me + d) % FS
            pltpu.make_async_remote_copy(
                src(peer), dst(me), send.at[sem, d], recv.at[sem, d], device_id={"fs": peer}, device_id_type=MESH
            ).start()

    def from_peers(src, dst, send, recv, sem):
        @pl.loop(1, FS)
        def _(d):
            peer = (me - d + FS) % FS
            pltpu.make_async_remote_copy(
                src(peer), dst(peer), send.at[sem, d], recv.at[sem, d], device_id={"fs": peer}, device_id_type=MESH
            ).wait_recv()

    def sent(src, dst, send, recv, sem):
        @pl.loop(1, FS)
        def _(d):
            peer = (me + d) % FS
            pltpu.make_async_remote_copy(
                src(peer), dst(me), send.at[sem, d], recv.at[sem, d], device_id={"fs": peer}, device_id_type=MESH
            ).wait_send()

    def part(ref, r, i):
        return ref.at[r, pl.ds(pl.multiple_of(SLICE * i, SLICE), SLICE), :]

    gx = (lambda p: gx_v.at[me], lambda i: gx_v.at[i], gx_send, gx_recv, 0)
    rs = [(functools.partial(part, lowp_v, r), lambda i, r=r: rs_v.at[r, i], rs_send, rs_recv, r) for r in range(ROLES)]
    ag = [(lambda p, r=r: part(low_v, r, me), functools.partial(part, low_v, r), ag_send, ag_recv, r) for r in range(ROLES)]
    gr = (lambda p: gp_v.at[p], lambda i: grs_v.at[i], gr_send, gr_recv, 0)
    ga = (lambda p: gfull_v.at[me], lambda i: gfull_v.at[i], ga_send, ga_recv, 0)

    facs = Gather(me, lambda i, h: fac_v.at[:, 2 * i + h, core], f_send, f_recv)
    fac_in[0].wait()
    fac_in[1].wait()
    facs.first()
    to_peers(*gx)

    def across(r, side):
        return pltpu.make_async_remote_copy(
            fac_v.at[r, :, side], fac_v.at[r, :, side], d_send.at[r], d_recv.at[r],
            device_id={"tp": tp + 1 - 2 * core}, device_id_type=MESH,
        )

    def turned(r, n):
        rows = pl.ds(pl.multiple_of(TURN * n, TURN), TURN)
        lhs_v[r % 2, 0:COLS, rows] = cot_v[r, rows, :].T

    def contract(r):
        fac = fac_v[r].reshape(DIM, RANK)
        both = jnp.dot(grad_v[r], fac, preferred_element_type=F32)
        low = (both[:COLS] + both[COLS:]).T
        lowp_v[r] = low
        to_peers(*rs[r])
        rs_v[r, me] = lowp_v[r, pl.ds(pl.multiple_of(SLICE * me, SLICE), SLICE), :]

    def reduce(r):
        from_peers(*rs[r])
        low_v[r, pl.ds(pl.multiple_of(SLICE * me, SLICE), SLICE), :] = jnp.sum(rs_v[r], axis=0)
        to_peers(*ag[r])

    def finish(r):
        low = low_v[r]
        first = BETA_ONE * fm_v[r] + (1.0 - BETA_ONE) * low
        second = BETA_TWO * sm_v[r] + (1.0 - BETA_TWO) * low * low
        first_ref[r] = first
        second_ref[r] = second
        direction = first * lax.rsqrt(second)
        squares = jnp.sum((direction * direction).reshape(RANK // 8, 8, COLS), axis=0)
        squares = squares[:, :128] + squares[:, 128:]
        sum_v[...] = squares if r == 0 else sum_v[...] + squares
        own = fac_v[r, pl.ds(2 * me, 2)].reshape(128, RANK)
        both = jnp.dot(own, jnp.concatenate(halves(direction), axis=1), preferred_element_type=F32)
        prod_v[r] = both[:, :COLS] + both[:, COLS:]

    cot_in[0].wait()

    @pl.loop(0, BLOCKS)
    def _(n):
        turned(0, n)

    for r in range(ROLES):
        rows = COLS + HEADS if r == 1 else COLS
        if r + 1 < ROLES:
            cot_in[r + 1].wait()

        @pl.loop(0, BLOCKS)
        def _(n):
            if r == 0:
                load(x_hbm.at[:, pl.ds(pl.multiple_of(BLOCK * n, BLOCK), BLOCK)], x_v.at[n], x_sem.at[n]).wait()
            grad = jnp.dot(lhs_v[r % 2, 0:rows, :], x_v[n], preferred_element_type=F32)
            if r + 1 < ROLES:
                turned(r + 1, n)
            upper, lower = halves(grad[:COLS])
            span = pl.ds(pl.multiple_of(BLOCK * n, BLOCK), BLOCK)
            grad_v[r, 0:COLS, span] = upper
            grad_v[r, COLS:, span] = lower
            if r == 1:
                for i in range(BLOCK // 128):
                    gp_v[(BLOCK // 128) * n + i] = grad[COLS:, 128 * i : 128 * i + 128]
            if r == 0:
                pl.when(n == 2)(facs.second)
            if r == 1:
                pl.when(n == 1)(facs.third)
            if r == 2:
                @pl.when(n == 1)
                def _():
                    across(0, 1 - core).wait_recv()
                    contract(0)

                @pl.when(n == 2)
                def _():
                    from_peers(*gr)
                    gfull_v[me] = jnp.sum(grs_v[...], axis=0)
                    to_peers(*ga)
                    across(1, 1 - core).wait_recv()
                    contract(1)

        if r == 0:
            from_peers(*gx)
            carried = jnp.zeros((HEADS, 1), F32)
            edge = jnp.zeros((HEADS, 1), F32)
            for i in range(FS):
                message = gx_v[i]
                carried = carried + jnp.where(i > me, message[:, 0:1], 0.0)
                edge = edge + jnp.where(i == me - 1, message[:, 64:65], 0.0)
            lhs_v[1, COLS:, :] = ((later_v[...] + carried) * gate_v[...]).astype(BF16)
            start = logs_v[:, 0:128]
            start = start - jnp.where(small == 0, edge, pltpu.roll(start, 1, 1))
            lhs_v[1, COLS:, 0:128] = ((later_v[:, 0:128] + carried) * minus_expm1(start)).astype(BF16)
        if r == 1:
            to_peers(*gr)
            grs_v[me] = gp_v[me]
            facs.last()
            for k in range(ROLES):
                across(k, core).start()

    across(2, 1 - core).wait_recv()
    contract(2)
    for c in rest_in:
        c.wait()
    reduce(0)
    reduce(1)
    from_peers(*ag[0])
    finish(0)
    reduce(2)

    from_peers(*ga)
    for i in range(FS):
        cut = slice(128 * i, 128 * i + 128)
        gate = gfull_v[i]
        first = BETA_ONE * gf_v[:, cut] + (1.0 - BETA_ONE) * gate
        second = BETA_TWO * gs_v[:, cut] + (1.0 - BETA_TWO) * gate * gate
        new = gm_v[:, cut] - LEARN * (first * lax.rsqrt(second))
        gfirst_ref[:, cut] = first
        gsecond_ref[:, cut] = second
        gnew_ref[:, cut] = new
        gcopy_ref[:, cut] = new.astype(BF16)

    from_peers(*ag[1])
    finish(1)
    from_peers(*ag[2])
    finish(2)

    ss_v[tp] = sum_v[...]

    def squares_to(peer, slot, d):
        return pltpu.make_async_remote_copy(
            ss_v.at[slot], ss_v.at[slot], ss_send.at[d], ss_recv.at[d], device_id={"tp": peer}, device_id_type=MESH
        )

    @pl.loop(1, TP)
    def _(d):
        squares_to((tp + d) % TP, tp, d).start()

    @pl.loop(1, TP)
    def _(d):
        peer = (tp - d + TP) % TP
        squares_to(peer, peer, d).wait_recv()

    total = jnp.sum(jnp.sum(ss_v[...], axis=0), keepdims=True)
    scale = lax.rsqrt(total * (1.0 / (ROLES * RANK * COLS * TP)) + 1e-06)
    for r in range(ROLES):
        step = scale * prod_v[r]
        new = master_v[r] - LEARN * step
        step_ref[r] = step
        new_ref[r] = new
        copy_ref[r, pl.ds(2 * me, 2)] = new.astype(BF16).reshape(2, 64, COLS)

    copies = Gather(me, lambda i, h: copy_ref.at[:, 2 * i + h], c_send, c_recv)
    copies.first()
    copies.second()
    copies.third()
    copies.last()

    @pl.loop(1, TP)
    def _(d):
        squares_to((tp + d) % TP, tp, d).wait_send()

    for k in range(ROLES):
        across(k, core).wait_send()
        sent(*rs[k])
        sent(*ag[k])
    sent(*gx)
    sent(*gr)
    sent(*ga)
    facs.drain()
    copies.drain()


def local(*args):
    shapes = (
        ((ROLES, 128, COLS), F32),
        ((ROLES, 128, COLS), F32),
        ((ROLES, 2 * FS, 64, COLS), BF16),
        ((ROLES, RANK, COLS), F32),
        ((ROLES, RANK, COLS), F32),
        ((HEADS, DIM), F32),
        ((HEADS, DIM), BF16),
        ((HEADS, DIM), F32),
        ((HEADS, DIM), F32),
    )
    vmem, dma = pltpu.VMEM, pltpu.SemaphoreType.DMA
    gates = vmem((HEADS, DIM), F32)
    moments = vmem((ROLES, RANK, COLS), F32)
    outs = pl.pallas_call(
        kernel,
        out_shape=[jax.ShapeDtypeStruct(s, d) for s, d in shapes],
        in_specs=[pl.BlockSpec(memory_space=pl.ANY)] * 11,
        out_specs=[pl.BlockSpec(memory_space=vmem)] * 9,
        scratch_shapes=[
            vmem((BLOCKS, TOK, BLOCK), BF16),
            vmem((ROLES, TOK, COLS), BF16),
            vmem((HEADS, TOK), F32),
            vmem((HEADS, TOK), F32),
            vmem((ROLES, 128, COLS), F32),
            vmem((ROLES, 2 * FS, 2, 32, RANK), BF16),
            moments, moments, gates, gates, gates,
            vmem((2, COLS + HEADS, TOK), BF16),
            vmem((ROLES, 2 * COLS, DIM), BF16),
            vmem((HEADS, TOK), F32),
            vmem((HEADS, TOK), F32),
            vmem((FS, HEADS, 128), F32),
            moments,
            vmem((ROLES, FS, SLICE, COLS), F32),
            moments,
            vmem((FS, HEADS, 128), F32),
            vmem((FS, HEADS, 128), F32),
            vmem((FS, HEADS, 128), F32),
            vmem((ROLES, 128, COLS), F32),
            vmem((8, 128), F32),
            vmem((TP, 8, 128), F32),
            dma((10,)), dma((BLOCKS,)), dma((ROLES,)),
            dma((1, FS)), dma((1, FS)),
            dma((ROLES, FS)), dma((ROLES, FS)), dma((ROLES, FS)), dma((ROLES, FS)),
            dma((1, FS)), dma((1, FS)), dma((1, FS)), dma((1, FS)),
            dma((TP,)), dma((TP,)),
            dma((2, 15)), dma((2, 15)), dma((ROLES,)), dma((ROLES,)), dma((2, 15)), dma((2, 15)),
        ],
        compiler_params=pltpu.CompilerParams(
            collective_id=0, has_side_effects=True, vmem_limit_bytes=56 * 1024 * 1024
        ),
    )(*args)
    outs = list(outs)
    outs[2] = outs[2].reshape(ROLES, DIM, COLS)
    return tuple(outs)


def solution(mesh):
    placed = (
        P("fs", None),
        P(None, "fs", "tp"),
        P(None, "fs"),
        P(None, "fs"),
        P(None, "fs", "tp"),
        P(None, "fs", None),
        P(None, None, "tp"),
        P(None, None, "tp"),
        P(),
        P(),
        P(),
    )
    return jax.shard_map(
        local,
        mesh=mesh,
        in_specs=placed,
        out_specs=(
            P(None, "fs", "tp"),
            P(None, "fs", "tp"),
            P(None, None, "tp"),
            P(None, None, "tp"),
            P(None, None, "tp"),
            P(),
            P(),
            P(),
            P(),
        ),
        check_vma=False,
    )
```

time: 208 us -> 94.5 us (0.45)
  Pallas kernels: 0 us -> 81.8 us
  waiting for transfers between devices: 72 us -> 0 us
  matrix products: 35.5 us -> 0 us
  blocking collectives: 28.6 us -> 0 us
  starting transfers between devices: 15.8 us -> 0 us
  local copies, waits for them, and re-layouts: 26.1 us -> 11.8 us
  between operations: 14.9 us -> 0.68 us
  other arithmetic: 13.5 us -> 0 us
    pallas_call x0 -> x1, Pallas kernels: none -> 81.8 us  [local(): pl.pallas_call(kernel, out_shape=[jax.ShapeDtypeStruct(s, d) for s, d in...]
    all_gather x2 -> x0, waiting for transfers between devices: 59.6 us -> none  [the longest x1 40.8 us: local(): lax.all_gather(proj_new.astype(jnp.bfloat16), 'fs', axis=1, tiled=True)]
    dot_general x5 -> x0, matrix products: 35.5 us -> none  [the longest x1 16.1 us: local(): jnp.einsum('td,rdk->rtk', saved_input, all_factors, preferred_element_typ...]
    all_to_all x2 -> x0, blocking collectives: 28.6 us -> none  [the longest x1 19.2 us: summed_on_arrival(): lax.all_to_all(parts, axis, split_axis=0, concat_axis=0, tiled=True)]
    all_to_all x2 -> x0, waiting for transfers between devices: 12.4 us -> none  [from_everyone(): return lax.all_to_all(copies, axis, split_axis=0, concat_axis=0, tiled=True)]
    all_to_all x2 -> x0, starting transfers between devices: 11.8 us -> none  [from_everyone(): return lax.all_to_all(copies, axis, split_axis=0, concat_axis=0, tiled=True)]
    rev x2 -> x0, local copies, waits for them, and re-layouts: 11.1 us -> none  [the longest x1 9.34 us: local(): jnp.flip(cache_cot, 1)]
    another operation x3 -> x0, other arithmetic: 4.9 us -> none
  transfers between devices with their start and end apart: 5 -> 0, of which waited for: 3 -> 0; matrix products, arithmetic and copies ran while one was open for 16% -> 0% of each run, Pallas kernels for 0% -> 0%
where the time goes in v1:
time: 94.5 us; the launch traced here: 94.4 us
  Pallas kernels  81.8 us (87%)
  local copies, waits for them, and re-layouts  11.8 us (12%)
    pallas_call x1, Pallas kernels, local(): pl.pallas_call(kernel, out_shape=[jax.ShapeDtypeStruct(s, d) for s, d in...  81.8 us
    unnamed x21, local copies, waits for them, and re-layouts  11.8 us

profile of v1, /device:TPU:0, one launch (start us, length us, event | category | flops | bytes accessed | tf_op | source)
XLA Modules:
  0.0 94.4 jit_solution(5055303994769613365)
XLA Ops:
  0.6 81.8 %shard_map.178 = (f32[3,128,256]{2,1,0:T(8,128)}, f32[3,128,256]{2,1,0:T(8,128)}, bf16[3,32,64,256]{3,2,1,0:T(8,128)(2,1)}, f32[3,256,256]{2,1,0:T(8,128)}, f32[...) custom-call(bf16[3072,2048]{1,0:T(8,128)(2,1)} %x_hbm.1, ...), custom_call_target="tpu_custom_call" | custom-call | tf_op jit(solution)/shard_map/pallas_call | solution.py:403
  82.5 0.0 copy-start.1
  82.5 0.0 copy-start
  82.5 1.9 %copy.29 = f32[3,128,256]{2,1,0:T(8,128)} copy(f32[3,128,256]{2,1,0:T(8,128)} %get-tuple-element.36) | data formatting | bytes 786432
  84.4 1.8 %copy.30 = f32[3,128,256]{2,1,0:T(8,128)} copy(f32[3,128,256]{2,1,0:T(8,128)} %get-tuple-element.37) | data formatting | bytes 786432
  86.2 0.0 copy-start.4
  86.2 0.0 copy-start.5
  86.2 0.0 copy-start.3
  86.2 0.0 copy-start.2
  86.2 3.8 %copy.31 = bf16[3,2048,256]{2,1,0:T(8,128)(2,1)} copy(bf16[3,2048,256]{2,1,0:T(8,128)(2,1)} %bitcast.1) | data formatting | bytes 6291456
  90.0 0.0 copy-done.1
  90.0 0.9 copy.32
  90.9 0.0 copy-done
  90.9 0.9 copy.33
  91.7 0.0 copy-done.4
  91.8 0.7 copy.34
  92.4 0.0 copy-done.5
  92.4 0.6 copy.35
  93.0 0.0 copy-done.3
  93.0 0.7 copy.36
  93.7 0.0 copy-done.2
  93.7 0.7 copy.37
Async XLA Ops:
  82.5 7.5 %copy-start.1 = (f32[3,256,256]{2,1,0:T(8,128)S(1)}, f32[3,256,256]{2,1,0:T(8,128)}, u32[]{:S(2)}) copy-start(f32[3,256,256]{2,1,0:T(8,128)} %get-tuple-element.39) | copy-start | bytes 2359300
  82.5 8.4 %copy-start = (f32[3,256,256]{2,1,0:T(8,128)S(1)}, f32[3,256,256]{2,1,0:T(8,128)}, u32[]{:S(2)}) copy-start(f32[3,256,256]{2,1,0:T(8,128)} %get-tuple-element.40) | copy-start | bytes 2359300
  86.2 5.6 %copy-start.4 = (f32[16,2048]{1,0:T(8,128)S(1)}, f32[16,2048]{1,0:T(8,128)}, u32[]{:S(2)}) copy-start(f32[16,2048]{1,0:T(8,128)} %get-tuple-element.41) | copy-start | bytes 393220
  86.2 6.2 %copy-start.5 = (bf16[16,2048]{1,0:T(8,128)(2,1)S(1)}, bf16[16,2048]{1,0:T(8,128)(2,1)}, u32[]{:S(2)}) copy-start(bf16[16,2048]{1,0:T(8,128)(2,1)} %get-tuple-element.42) | copy-start | bytes 196612
  86.2 6.9 %copy-start.3 = (f32[16,2048]{1,0:T(8,128)S(1)}, f32[16,2048]{1,0:T(8,128)}, u32[]{:S(2)}) copy-start(f32[16,2048]{1,0:T(8,128)} %get-tuple-element.43) | copy-start | bytes 393220
  86.2 7.5 %copy-start.2 = (f32[16,2048]{1,0:T(8,128)S(1)}, f32[16,2048]{1,0:T(8,128)}, u32[]{:S(2)}) copy-start(f32[16,2048]{1,0:T(8,128)} %get-tuple-element.44) | copy-start | bytes 393220

commit v2 on v1

v2 whole, which is shorter than its diff:
```python
import functools

import jax
import jax.numpy as jnp
from jax import lax
from jax.experimental import pallas as pl
from jax.experimental.pallas import tpu as pltpu
from jax.sharding import PartitionSpec as P

BETA_ONE = 0.8
BETA_TWO = 0.9
LEARN = 0.001
MESH = pl.DeviceIdType.MESH
F32, BF16 = jnp.float32, jnp.bfloat16

FS, TP, RING = 16, 8, 4
ROLES, TOK, DIM, COLS, RANK, HEADS = 3, 3072, 2048, 256, 256, 16
BLOCK = 512
BLOCKS = DIM // BLOCK
TURN = TOK // BLOCKS


def minus_expm1(x):
    series = jnp.ones_like(x)
    for n in range(9, 1, -1):
        series = 1.0 + x * (1.0 / n) * series
    return jnp.where(jnp.abs(x) < 0.5, -x * series, 1.0 - jnp.exp(x))


def halves(x):
    upper = x.astype(BF16)
    return upper, (x - upper.astype(F32)).astype(BF16)


class Gather:
    def __init__(self, me, piece, many, send, recv):
        self.me, self.piece, self.many, self.send, self.recv = me, piece, many, send, recv
        x, z = me % RING, me // RING
        self.at = ((x, z), (z, x))

    def name(self, half, first, second):
        return second * RING + first if half == 0 else first * RING + second

    def sem(self, half, index):
        if index < 3:
            return self.recv.at[7 * half + index]
        e, kind = divmod(index - 3, 3)
        if kind == (0 if e == 0 else 1):
            return self.recv.at[7 * half + 3 + e]
        return self.recv.at[14]

    def copy(self, half, index):
        p, q = self.at[half]
        turn = lambda a, b: (a + b + RING) % RING
        if index < 3:
            d = index + 1
            out, to, came = (p, q), (turn(p, d), q), (turn(p, -d), q)
        else:
            e, kind = divmod(index - 3, 3)
            first = turn(p, -e)
            if kind == 0:
                out, to, came = (first, q), (p, turn(q, 1)), (first, turn(q, -1))
            elif kind == 1:
                out, to, came = (first, q), (p, turn(q, -1)), (first, turn(q, 1))
            elif e == 0:
                out, to, came = (first, turn(q, -1)), (p, turn(q, 1)), (first, turn(q, 2))
            else:
                out, to, came = (first, turn(q, 1)), (p, turn(q, -1)), (first, turn(q, 2))
        ref = self.piece(self.name(half, *out), half)
        got = self.piece(self.name(half, *came), half)
        to = {"fs": self.name(half, *to)}
        make = lambda r: pltpu.make_async_remote_copy(
            r, r, self.send, self.sem(half, index), device_id=to, device_id_type=MESH
        )
        return make(ref), make(got)

    def start(self, half, index):
        self.copy(half, index)[0].start()

    def arrived(self, half, index):
        self.copy(half, index)[1].wait_recv()

    def first(self):
        for index in (1, 0, 2, 3, 4):
            for half in (0, 1):
                self.start(half, index)

    def second(self):
        for half in (0, 1):
            self.arrived(half, 3)
            self.start(half, 5)
        for e in (1, 3, 2):
            for half in (0, 1):
                self.arrived(half, e - 1)
                self.start(half, 3 + 3 * e)
                self.start(half, 4 + 3 * e)

    def third(self):
        for e in (1, 3, 2):
            for half in (0, 1):
                self.arrived(half, 4 + 3 * e)
                self.start(half, 5 + 3 * e)

    def whole(self, n, sem):
        ref = self.many(n)
        return pltpu.make_async_remote_copy(
            ref, ref, self.send, sem, device_id={"fs": (self.me + 1) % FS}, device_id_type=MESH
        )

    def last(self):
        self.whole(16, self.recv.at[14]).wait_recv()

    def drain(self):
        self.whole(30, self.recv.at[14]).wait_send()


def kernel(
    x_hbm, cot_hbm, logs_hbm, ccot_hbm, master_hbm, factors_hbm, first_hbm, second_hbm, gm_hbm, gf_hbm, gs_hbm,
    step_ref, new_ref, copy_ref, first_ref, second_ref, gnew_ref, gcopy_ref, gfirst_ref, gsecond_ref,
    x_v, cot_v, logs_v, ccot_v, master_v, fac_v, fm_v, sm_v, gm_v, gf_v, gs_v,
    lhs_v, grad_v, later_v, gate_v, gx_v, lowp_v, sum_a, sum_b, sum_c, low_v, gp_v, grs_v, gfull_v, prod_v, ss_v, st_v,
    in_sem, x_sem, cot_sem, p_send, p_recv, s_send, s_recv, ss_sem, f_send, f_recv, d_send, d_recv, c_send, c_recv,
):
    me, tp = lax.axis_index("fs"), lax.axis_index("tp")
    core = tp % 2

    def load(src, dst, sem):
        return pltpu.make_async_copy(src, dst, sem)

    fac_in = [
        load(factors_hbm.at[:, pl.ds(pl.multiple_of(64 * h + 32 * core, 32), 32), :], fac_v.at[:, 2 * me + h, core], in_sem.at[h])
        for h in (0, 1)
    ]
    logs_in = load(logs_hbm, logs_v, in_sem.at[2])
    ccot_in = load(ccot_hbm, ccot_v, in_sem.at[3])
    cot_in = [load(cot_hbm.at[r], cot_v.at[r], cot_sem.at[r]) for r in range(ROLES)]
    x_in = [load(x_hbm.at[:, pl.ds(BLOCK * n, BLOCK)], x_v.at[n], x_sem.at[n]) for n in range(BLOCKS)]
    rest_in = [
        load(s, d, in_sem.at[4 + i])
        for i, (s, d) in enumerate(
            ((first_hbm, fm_v), (second_hbm, sm_v), (master_hbm, master_v), (gm_hbm, gm_v), (gf_hbm, gf_v), (gs_hbm, gs_v))
        )
    ]
    for c in (*fac_in, ccot_in, logs_in, cot_in[0], x_in[0], cot_in[1], *x_in[1:], cot_in[2], *rest_in):
        c.start()

    barrier = pltpu.get_barrier_semaphore()

    @pl.loop(1, FS)
    def _(d):
        pl.semaphore_signal(barrier, inc=1, device_id={"fs": (me + d) % FS}, device_id_type=MESH)

    @pl.loop(1, TP)
    def _(d):
        pl.semaphore_signal(barrier, inc=1, device_id={"tp": (tp + d) % TP}, device_id_type=MESH)

    def put(src, dst, send, recv, to):
        return pltpu.make_async_remote_copy(src, dst, send, recv, device_id=to, device_id_type=MESH)

    def to_peers(src, dst, k):
        @pl.loop(1, FS)
        def _(d):
            peer = (me + d) % FS
            put(src(peer), dst, p_send.at[k], p_recv.at[k], {"fs": peer}).start()

    def from_peers(ref, k):
        ref = ref.at[pl.ds(0, FS - 1)]
        put(ref, ref, p_send.at[k], p_recv.at[k], {"fs": (me + 1) % FS}).wait_recv()

    def sent(ref, k):
        ref = ref.at[pl.ds(0, FS - 1)]
        put(ref, ref, p_send.at[k], p_recv.at[k], {"fs": (me + 1) % FS}).wait_send()

    me_x, me_z = me % RING, me // RING
    at = ((me_x, me_z), (me_z, me_x))

    def device(half, first, second):
        return {"fs": second * RING + first if half == 0 else first * RING + second}

    def turn(a, d):
        return (a + d) % RING

    def rows(start, size):
        return pl.ds(pl.multiple_of(start, 8), size)

    def swap(r, phase):
        for half in (0, 1):
            p, q = at[half]
            for d in (1, 3, 2):
                if phase == 0:
                    to = (turn(p, d), q)
                    src = lowp_v.at[r, rows(128 * half + 32 * to[0], 32)]
                    dst = sum_a.at[r, half, d - 1]
                elif phase == 1:
                    to = (p, turn(q, d))
                    src = sum_b.at[r, half, rows(8 * to[1], 8)]
                    dst = sum_c.at[r, half, d - 1]
                elif phase == 2:
                    to = (p, turn(q, d))
                    src = dst = low_v.at[r, rows(128 * half + 32 * p + 8 * q, 8)]
                else:
                    to = (turn(p, d), q)
                    src = dst = low_v.at[r, rows(128 * half + 32 * p, 32)]
                put(src, dst, s_send.at[r, phase], s_recv.at[r, phase], device(half, *to)).start()

    def whole(r, phase):
        ref = (sum_a.at[r], sum_c.at[r], low_v.at[r, pl.ds(0, 48)], low_v.at[r, pl.ds(0, 192)])[phase]
        return put(ref, ref, s_send.at[r, phase], s_recv.at[r, phase], {"fs": (me + 1) % FS})

    def second_sum(r):
        whole(r, 0).wait_recv()
        for half in (0, 1):
            p, q = at[half]
            got = sum_a[r, half]
            sum_b[r, half] = lowp_v[r, rows(128 * half + 32 * p, 32)] + got[0] + got[1] + got[2]
        swap(r, 1)

    def first_spread(r):
        whole(r, 1).wait_recv()
        for half in (0, 1):
            p, q = at[half]
            got = sum_c[r, half]
            low_v[r, rows(128 * half + 32 * p + 8 * q, 8)] = sum_b[r, half, rows(8 * q, 8)] + got[0] + got[1] + got[2]
        swap(r, 2)

    def second_spread(r):
        whole(r, 2).wait_recv()
        swap(r, 3)

    ccot_in.wait()
    logs_in.wait()
    small = lax.broadcasted_iota(jnp.int32, (8, 128), 1)
    sums = jnp.sum(ccot_v[...], axis=1, keepdims=True)
    ends = logs_v[:, TOK - 128 :][:, 127:128]
    message = jnp.where(small < 32, sums[:8], sums[8:])
    message = jnp.where(small < 64, message, ends[:8])
    gx_v[me] = jnp.where(small < 96, message, ends[8:])

    facs = [
        Gather(
            me,
            lambda i, h, r=r: fac_v.at[r, 2 * i + h, core],
            lambda n, r=r: fac_v.at[r, pl.ds(0, n), core],
            f_send.at[r],
            f_recv.at[r],
        )
        for r in range(ROLES)
    ]
    fac_in[0].wait()
    fac_in[1].wait()
    pl.semaphore_wait(barrier, FS + TP - 2)
    to_peers(lambda peer: gx_v.at[me], gx_v.at[me], 0)
    for r in range(ROLES):
        facs[r].first()

    lane = lax.broadcasted_iota(jnp.int32, (HEADS, TOK), 1)
    later = ccot_v[...]
    by = 1
    while by < TOK:
        later = later + jnp.where(lane < TOK - by, pltpu.roll(later, TOK - by, 1), 0.0)
        by *= 2
    later_v[...] = later
    logs = logs_v[...]
    gate_v[...] = minus_expm1(logs - pltpu.roll(logs, 1, 1))

    def across(r, side):
        return pltpu.make_async_remote_copy(
            fac_v.at[r, :, side], fac_v.at[r, :, side], d_send.at[r], d_recv.at[r],
            device_id={"tp": tp + 1 - 2 * core}, device_id_type=MESH,
        )

    def turned(r, n):
        span = pl.ds(pl.multiple_of(TURN * n, TURN), TURN)
        lhs_v[r % 2, 0:COLS, span] = cot_v[r, span, :].T

    def contract(r):
        fac = fac_v[r].reshape(DIM, RANK)
        both = jnp.dot(grad_v[r], fac, preferred_element_type=F32)
        lowp_v[r] = (both[:COLS] + both[COLS:]).T
        swap(r, 0)

    def finish(r):
        low = low_v[r]
        first = BETA_ONE * fm_v[r] + (1.0 - BETA_ONE) * low
        second = BETA_TWO * sm_v[r] + (1.0 - BETA_TWO) * low * low
        first_ref[r] = first
        second_ref[r] = second
        direction = first * lax.rsqrt(second)
        own = fac_v[r, pl.ds(2 * me, 2)].reshape(128, RANK)
        both = jnp.dot(own, jnp.concatenate(halves(direction), axis=1), preferred_element_type=F32)
        prod_v[r] = both[:, :COLS] + both[:, COLS:]

    cot_in[0].wait()

    @pl.loop(0, BLOCKS)
    def _(n):
        turned(0, n)

    def handed(r):
        facs[r].last()
        across(r, core).start()

    def joined(r):
        across(r, 1 - core).wait_recv()
        contract(r)

    events = (
        ((1, facs[0].second), (2, facs[1].second), (3, facs[2].second)),
        (
            (0, facs[0].third),
            (1, facs[1].third),
            (2, facs[2].third),
            (2, functools.partial(handed, 0)),
            (3, functools.partial(handed, 1)),
        ),
        ((0, functools.partial(handed, 2)), (1, functools.partial(joined, 0)), (2, functools.partial(joined, 1))),
    )

    for r in range(ROLES):
        height = COLS + HEADS if r == 1 else COLS

        @pl.loop(0, BLOCKS)
        def _(n):
            if r == 0:
                load(x_hbm.at[:, pl.ds(pl.multiple_of(BLOCK * n, BLOCK), BLOCK)], x_v.at[n], x_sem.at[n]).wait()
            grad = jnp.dot(lhs_v[r % 2, 0:height, :], x_v[n], preferred_element_type=F32)
            if r + 1 < ROLES:
                pl.when(n == 0)(cot_in[r + 1].wait)
                turned(r + 1, n)
            upper, lower = halves(grad[:COLS])
            span = pl.ds(pl.multiple_of(BLOCK * n, BLOCK), BLOCK)
            grad_v[r, 0:COLS, span] = upper
            grad_v[r, COLS:, span] = lower
            if r == 1:
                for i in range(BLOCK // 128):
                    gp_v[(BLOCK // 128) * n + i] = grad[COLS:, 128 * i : 128 * i + 128]
            for event, work in events[r]:
                pl.when(n == event)(work)

        if r == 0:
            from_peers(gx_v, 0)
            carried = jnp.zeros((8, 128), F32)
            edge = jnp.zeros((8, 128), F32)
            for i in range(FS):
                message = gx_v[i]
                carried = carried + jnp.where(i > me, message, 0.0)
                edge = edge + jnp.where(i == me - 1, message, 0.0)
            carried = jnp.concatenate([carried[:, 0:1], carried[:, 32:33]], axis=0)
            edge = jnp.concatenate([edge[:, 64:65], edge[:, 96:97]], axis=0)
            lhs_v[1, COLS:, :] = ((later_v[...] + carried) * gate_v[...]).astype(BF16)
            start = logs_v[:, 0:128]
            start = start - jnp.where(lane[:, 0:128] == 0, edge, pltpu.roll(start, 1, 1))
            lhs_v[1, COLS:, 0:128] = ((later_v[:, 0:128] + carried) * minus_expm1(start)).astype(BF16)
        if r == 1:
            to_peers(lambda peer: gp_v.at[peer], grs_v.at[me], 1)
            grs_v[me] = gp_v[me]

    joined(2)
    for c in rest_in:
        c.wait()

    def slice_squares(r):
        squares = jnp.zeros((8, COLS), F32)
        for half in (0, 1):
            p, q = at[half]
            own = rows(128 * half + 32 * p + 8 * q, 8)
            low = low_v[r, own]
            first = BETA_ONE * fm_v[r, own] + (1.0 - BETA_ONE) * low
            second = BETA_TWO * sm_v[r, own] + (1.0 - BETA_TWO) * low * low
            direction = first * lax.rsqrt(second)
            squares = squares + direction * direction
        return squares[:, :128] + squares[:, 128:]

    from_peers(grs_v, 1)
    gfull_v[me] = jnp.sum(grs_v[...], axis=0)
    second_sum(0)
    second_sum(1)
    first_spread(0)
    second_sum(2)
    first_spread(1)
    second_spread(0)
    first_spread(2)

    ss_v[tp] = slice_squares(0) + slice_squares(1) + slice_squares(2)

    @pl.loop(1, TP)
    def _(d):
        put(ss_v.at[tp], ss_v.at[tp], ss_sem.at[0], ss_sem.at[1], {"tp": (tp + d) % TP}).start()

    squares = put(ss_v.at[pl.ds(0, TP - 1)], ss_v.at[pl.ds(0, TP - 1)], ss_sem.at[0], ss_sem.at[1], {"tp": (tp + 1) % TP})
    to_peers(lambda peer: gfull_v.at[me], gfull_v.at[me], 2)
    second_spread(1)
    squares.wait_recv()
    st_v[me] = jnp.sum(ss_v[...], axis=0)
    to_peers(lambda peer: st_v.at[me], st_v.at[me], 3)
    second_spread(2)
    whole(0, 3).wait_recv()
    finish(0)
    whole(1, 3).wait_recv()
    finish(1)
    whole(2, 3).wait_recv()
    finish(2)

    from_peers(st_v, 3)
    total = jnp.sum(jnp.sum(st_v[...], axis=0), keepdims=True)
    scale = lax.rsqrt(total * (1.0 / (ROLES * RANK * COLS * TP)) + 1e-06)
    copies = [
        Gather(
            me, lambda i, h, r=r: copy_ref.at[r, 2 * i + h], lambda n, r=r: copy_ref.at[r, pl.ds(0, n)], c_send.at[r], c_recv.at[r]
        )
        for r in range(ROLES)
    ]
    for r in range(ROLES):
        step = scale * prod_v[r]
        new = master_v[r] - LEARN * step
        step_ref[r] = step
        new_ref[r] = new
        copy_ref[r, pl.ds(2 * me, 2)] = new.astype(BF16).reshape(2, 64, COLS)
        copies[r].first()

    from_peers(gfull_v, 2)
    for i in range(FS):
        cut = slice(128 * i, 128 * i + 128)
        gate = gfull_v[i]
        first = BETA_ONE * gf_v[:, cut] + (1.0 - BETA_ONE) * gate
        second = BETA_TWO * gs_v[:, cut] + (1.0 - BETA_TWO) * gate * gate
        new = gm_v[:, cut] - LEARN * (first * lax.rsqrt(second))
        gfirst_ref[:, cut] = first
        gsecond_ref[:, cut] = second
        gnew_ref[:, cut] = new
        gcopy_ref[:, cut] = new.astype(BF16)
    squares.wait_send()
    for r in range(ROLES):
        across(r, core).wait_send()
        for phase in range(4):
            whole(r, phase).wait_send()
    sent(gx_v, 0)
    sent(gp_v, 1)
    sent(gfull_v, 2)
    sent(st_v, 3)
    for r in range(ROLES):
        facs[r].drain()

    for step in ("second", "third", "last", "drain"):
        for gather in copies:
            getattr(gather, step)()


def written(*refs):
    copies = [pltpu.make_async_copy(refs[i], refs[9 + i], refs[18].at[i]) for i in range(9)]
    for c in copies:
        c.start()
    for c in copies:
        c.wait()


def local(*args):
    shapes = (
        ((ROLES, 128, COLS), F32),
        ((ROLES, 128, COLS), F32),
        ((ROLES, 2 * FS, 64, COLS), BF16),
        ((ROLES, RANK, COLS), F32),
        ((ROLES, RANK, COLS), F32),
        ((HEADS, DIM), F32),
        ((HEADS, DIM), BF16),
        ((HEADS, DIM), F32),
        ((HEADS, DIM), F32),
    )
    vmem, dma = pltpu.VMEM, pltpu.SemaphoreType.DMA
    gates = vmem((HEADS, DIM), F32)
    moments = vmem((ROLES, RANK, COLS), F32)
    outs = pl.pallas_call(
        kernel,
        out_shape=[vmem(s, d) for s, d in shapes],
        in_specs=[pl.BlockSpec(memory_space=pl.ANY)] * 11,
        out_specs=[pl.BlockSpec(memory_space=vmem)] * 9,
        scratch_shapes=[
            vmem((BLOCKS, TOK, BLOCK), BF16),
            vmem((ROLES, TOK, COLS), BF16),
            vmem((HEADS, TOK), F32),
            vmem((HEADS, TOK), F32),
            vmem((ROLES, 128, COLS), F32),
            vmem((ROLES, 2 * FS, 2, 32, RANK), BF16),
            moments, moments, gates, gates, gates,
            vmem((2, COLS + HEADS, TOK), BF16),
            vmem((ROLES, 2 * COLS, DIM), BF16),
            vmem((HEADS, TOK), F32),
            vmem((HEADS, TOK), F32),
            vmem((FS, 8, 128), F32),
            moments,
            vmem((ROLES, 2, 3, 32, COLS), F32),
            vmem((ROLES, 2, 32, COLS), F32),
            vmem((ROLES, 2, 3, 8, COLS), F32),
            moments,
            vmem((FS, HEADS, 128), F32),
            vmem((FS, HEADS, 128), F32),
            vmem((FS, HEADS, 128), F32),
            vmem((ROLES, 128, COLS), F32),
            vmem((TP, 8, 128), F32),
            vmem((FS, 8, 128), F32),
            dma((10,)), dma((BLOCKS,)), dma((ROLES,)),
            dma((4,)), dma((4,)), dma((ROLES, 4)), dma((ROLES, 4)), dma((2,)),
            dma((ROLES,)), dma((ROLES, 15)), dma((ROLES,)), dma((ROLES,)), dma((ROLES,)), dma((ROLES, 15)),
        ],
        compiler_params=pltpu.CompilerParams(
            collective_id=0, has_side_effects=True, vmem_limit_bytes=57 * 1024 * 1024
        ),
    )(*args)
    outs = pl.pallas_call(
        written,
        out_shape=[jax.ShapeDtypeStruct(s, d) for s, d in shapes],
        in_specs=[pl.BlockSpec(memory_space=vmem)] * 9,
        out_specs=[pl.BlockSpec(memory_space=pl.ANY)] * 9,
        scratch_shapes=[dma((9,))],
        compiler_params=pltpu.CompilerParams(vmem_limit_bytes=1024 * 1024),
    )(*(pltpu.with_memory_space_constraint(o, pltpu.VMEM) for o in outs))
    outs = list(outs)
    outs[2] = outs[2].reshape(ROLES, DIM, COLS)
    return tuple(outs)


def solution(mesh):
    placed = (
        P("fs", None),
        P(None, "fs", "tp"),
        P(None, "fs"),
        P(None, "fs"),
        P(None, "fs", "tp"),
        P(None, "fs", None),
        P(None, None, "tp"),
        P(None, None, "tp"),
        P(),
        P(),
        P(),
    )
    return jax.shard_map(
        local,
        mesh=mesh,
        in_specs=placed,
        out_specs=(
            P(None, "fs", "tp"),
            P(None, "fs", "tp"),
            P(None, None, "tp"),
            P(None, None, "tp"),
            P(None, None, "tp"),
            P(),
            P(),
            P(),
            P(),
        ),
        check_vma=False,
    )
```

time: 94.5 us -> 71.8 us (0.76)
  local copies, waits for them, and re-layouts: 11.8 us -> 0 us
  Pallas kernels: 81.8 us -> 70.7 us
    unnamed x21 -> x0, local copies, waits for them, and re-layouts: 11.8 us -> none
    pallas_call x1 -> x2, Pallas kernels: 81.8 us -> 70.7 us  [the longest x1 68.1 us: local(): pl.pallas_call(kernel, out_shape=[vmem(s, d) for s, d in shapes], in_spec...]
where the time goes in v2:
time: 71.8 us; the launch traced here: 71.4 us
  Pallas kernels  70.7 us (98%)
    pallas_call x1, Pallas kernels, local(): pl.pallas_call(kernel, out_shape=[vmem(s, d) for s, d in shapes], in_spec...  68.1 us
    pallas_call x1, Pallas kernels, local(): pl.pallas_call(written, out_shape=[jax.ShapeDtypeStruct(s, d) for s, d in...  2.63 us

profile of v2, /device:TPU:0, one launch (start us, length us, event | category | flops | bytes accessed | tf_op | source)
XLA Modules:
  0.0 71.4 jit_solution(15780844454447332076)
XLA Ops:
  0.6 68.1 %shard_map.178 = (f32[3,128,256]{2,1,0:T(8,128)S(1)}, f32[3,128,256]{2,1,0:T(8,128)S(1)}, bf16[3,32,64,256]{3,2,1,0:T(8,128)(2,1)S(1)}, f32[3,256,256]{2,1,0:T(8...) custom-call(bf16[3072,2048]{1,0:T(8,128)(2,1)} %x_hbm.1, ...), custom_call_target="tpu_custom_call" | custom-call | tf_op jit(solution)/shard_map/pallas_call | solution.py:472
  68.8 2.6 %shard_map.179 = (f32[3,128,256]{2,1,0:T(8,128)}, f32[3,128,256]{2,1,0:T(8,128)}, bf16[3,32,64,256]{3,2,1,0:T(8,128)(2,1)}, f32[3,256,256]{2,1,0:T(8,128)}, f32[...) custom-call(f32[3,128,256]{2,1,0:T(8,128)S(1)} %get-tuple-element.27, ...), custom_call_target="tpu_custom_call" | custom-call | tf_op jit(solution)/shard_map/pallas_call | solution.py:509

commit v3 on v2

--- a/solution.py
+++ b/solution.py
@@ -17,6 +17,7 @@
 ROLES, TOK, DIM, COLS, RANK, HEADS = 3, 3072, 2048, 256, 256, 16
 BLOCK = 512
 BLOCKS = DIM // BLOCK
+EARLY = 16
 TURN = TOK // BLOCKS
 
 
@@ -33,73 +34,75 @@
 
 
 class Gather:
-    def __init__(self, me, piece, many, send, recv):
-        self.me, self.piece, self.many, self.send, self.recv = me, piece, many, send, recv
+    def __init__(self, me, piece, many, send, recv, coarse=False):
+        self.me, self.piece, self.many, self.send, self.recv, self.coarse = me, piece, many, send, recv, coarse
         x, z = me % RING, me // RING
         self.at = ((x, z), (z, x))
 
     def name(self, half, first, second):
         return second * RING + first if half == 0 else first * RING + second
 
-    def sem(self, half, index):
+    def sem(self, index):
         if index < 3:
-            return self.recv.at[7 * half + index]
+            return self.recv.at[1 if self.coarse else 1 + index]
         e, kind = divmod(index - 3, 3)
-        if kind == (0 if e == 0 else 1):
-            return self.recv.at[7 * half + 3 + e]
-        return self.recv.at[14]
+        if kind == (0 if e < 2 else 1):
+            return self.recv.at[(1 if e == 0 else 2) if self.coarse else 4 + e]
+        return self.recv.at[0]
 
     def copy(self, half, index):
         p, q = self.at[half]
         turn = lambda a, b: (a + b + RING) % RING
         if index < 3:
             d = index + 1
-            out, to, came = (p, q), (turn(p, d), q), (turn(p, -d), q)
+            out, to = (p, q), (turn(p, d), q)
         else:
             e, kind = divmod(index - 3, 3)
             first = turn(p, -e)
             if kind == 0:
-                out, to, came = (first, q), (p, turn(q, 1)), (first, turn(q, -1))
+                out, to = (first, q), (p, turn(q, 1))
             elif kind == 1:
-                out, to, came = (first, q), (p, turn(q, -1)), (first, turn(q, 1))
-            elif e == 0:
-                out, to, came = (first, turn(q, -1)), (p, turn(q, 1)), (first, turn(q, 2))
+                out, to = (first, q), (p, turn(q, -1))
+            elif e < 2:
+                out, to = (first, turn(q, -1)), (p, turn(q, 1))
             else:
-                out, to, came = (first, turn(q, 1)), (p, turn(q, -1)), (first, turn(q, 2))
+                out, to = (first, turn(q, 1)), (p, turn(q, -1))
         ref = self.piece(self.name(half, *out), half)
-        got = self.piece(self.name(half, *came), half)
-        to = {"fs": self.name(half, *to)}
-        make = lambda r: pltpu.make_async_remote_copy(
-            r, r, self.send, self.sem(half, index), device_id=to, device_id_type=MESH
+        return pltpu.make_async_remote_copy(
+            ref, ref, self.send, self.sem(index), device_id={"fs": self.name(half, *to)}, device_id_type=MESH
         )
-        return make(ref), make(got)
-
-    def start(self, half, index):
-        self.copy(half, index)[0].start()
-
-    def arrived(self, half, index):
-        self.copy(half, index)[1].wait_recv()
+
+    def start(self, index):
+        for half in (0, 1):
+            self.copy(half, index).start()
+
+    def arrived(self, index):
+        self.whole(2, self.sem(index)).wait_recv()
 
     def first(self):
         for index in (1, 0, 2, 3, 4):
-            for half in (0, 1):
-                self.start(half, index)
-
-    def second(self):
-        for half in (0, 1):
-            self.arrived(half, 3)
-            self.start(half, 5)
+            self.start(index)
+
+    def second(self, own=True, behind=(1, 3, 2)):
+        if self.coarse:
+            self.whole(8, self.recv.at[1]).wait_recv()
+        if own:
+            if not self.coarse:
+                self.arrived(3)
+            self.start(5)
+        for e in behind:
+            if not self.coarse:
+                self.arrived(e - 1)
+            self.start(3 + 3 * e)
+            self.start(4 + 3 * e)
+
+    def third(self):
+        if self.coarse:
+            self.whole(6, self.recv.at[2]).wait_recv()
         for e in (1, 3, 2):
-            for half in (0, 1):
-                self.arrived(half, e - 1)
-                self.start(half, 3 + 3 * e)
-                self.start(half, 4 + 3 * e)
-
-    def third(self):
-        for e in (1, 3, 2):
-            for half in (0, 1):
-                self.arrived(half, 4 + 3 * e)
-                self.start(half, 5 + 3 * e)
+            if not self.coarse:
+                self.arrived(3 + 3 * e if e < 2 else 4 + 3 * e)
+            self.start(5 + 3 * e)
 
     def whole(self, n, sem):
         ref = self.many(n)
@@ -108,18 +111,18 @@
         )
 
     def last(self):
-        self.whole(16, self.recv.at[14]).wait_recv()
+        self.whole(16, self.recv.at[0]).wait_recv()
 
     def drain(self):
-        self.whole(30, self.recv.at[14]).wait_send()
+        self.whole(30, self.recv.at[0]).wait_send()
 
 
 def kernel(
     x_hbm, cot_hbm, logs_hbm, ccot_hbm, master_hbm, factors_hbm, first_hbm, second_hbm, gm_hbm, gf_hbm, gs_hbm,
     step_ref, new_ref, copy_ref, first_ref, second_ref, gnew_ref, gcopy_ref, gfirst_ref, gsecond_ref,
     x_v, cot_v, logs_v, ccot_v, master_v, fac_v, fm_v, sm_v, gm_v, gf_v, gs_v,
-    lhs_v, grad_v, later_v, gate_v, gx_v, lowp_v, sum_a, sum_b, sum_c, low_v, gp_v, grs_v, gfull_v, prod_v, ss_v, st_v,
-    in_sem, x_sem, cot_sem, p_send, p_recv, s_send, s_recv, ss_sem, f_send, f_recv, d_send, d_recv, c_send, c_recv,
+    lhs_v, grad_v, later_v, gate_v, gx_v, lowp_v, sum_a, sum_b, sum_c, low_v, gp_v, grs_v, gfull_v, prod_v, ss_v, st_v, early_v, dir_v,
+    in_sem, x_sem, cot_sem, p_send, p_recv, s_send, s_recv, ss_sem, f_send, f_recv, d_send, d_recv, c_send, c_recv, e_send, e_recv,
 ):
     me, tp = lax.axis_index("fs"), lax.axis_index("tp")
     core = tp % 2
@@ -141,7 +144,8 @@
             ((first_hbm, fm_v), (second_hbm, sm_v), (master_hbm, master_v), (gm_hbm, gm_v), (gf_hbm, gf_v), (gs_hbm, gs_v))
         )
     ]
-    for c in (*fac_in, ccot_in, logs_in, cot_in[0], x_in[0], cot_in[1], *x_in[1:], cot_in[2], *rest_in):
+    early_in = [load(master_hbm.at[:, pl.ds(64 * h, EARLY), :], early_v.at[:, 2 * me + h], in_sem.at[10 + h]) for h in (0, 1)]
+    for c in (*fac_in, ccot_in, logs_in, cot_in[0], x_in[0], cot_in[1], *x_in[1:], cot_in[2], *early_in, *rest_in):
         c.start()
 
     barrier = pltpu.get_barrier_semaphore()
@@ -201,11 +205,11 @@
                 else:
                     to = (turn(p, d), q)
                     src = dst = low_v.at[r, rows(128 * half + 32 * p, 32)]
-                put(src, dst, s_send.at[r, phase], s_recv.at[r, phase], device(half, *to)).start()
+                put(src, dst, s_send.at[r], s_recv.at[r, phase], device(half, *to)).start()
 
     def whole(r, phase):
         ref = (sum_a.at[r], sum_c.at[r], low_v.at[r, pl.ds(0, 48)], low_v.at[r, pl.ds(0, 192)])[phase]
-        return put(ref, ref, s_send.at[r, phase], s_recv.at[r, phase], {"fs": (me + 1) % FS})
+        return put(ref, ref, s_send.at[r], s_recv.at[r, phase], {"fs": (me + 1) % FS})
 
     def second_sum(r):
         whole(r, 0).wait_recv()
@@ -243,6 +247,7 @@
             lambda n, r=r: fac_v.at[r, pl.ds(0, n), core],
             f_send.at[r],
             f_recv.at[r],
+            True,
         )
         for r in range(ROLES)
     ]
@@ -269,6 +274,19 @@
             device_id={"tp": tp + 1 - 2 * core}, device_id_type=MESH,
         )
 
+    early = Gather(
+        me, lambda i, h: early_v.at[:, 2 * i + h], lambda n: early_v.at[:, pl.ds(0, n)], e_send.at[0], e_recv
+    )
+
+    def early_first():
+        for c in early_in:
+            c.wait()
+        early.first()
+
+    def other_gates(side):
+        ref = gfull_v.at[:, side]
+        return put(ref, ref, d_send.at[ROLES], d_recv.at[ROLES], {"tp": tp + 1 - 2 * core})
+
     def turned(r, n):
         span = pl.ds(pl.multiple_of(TURN * n, TURN), TURN)
         lhs_v[r % 2, 0:COLS, span] = cot_v[r, span, :].T
@@ -287,8 +305,15 @@
         second_ref[r] = second
         direction = first * lax.rsqrt(second)
         own = fac_v[r, pl.ds(2 * me, 2)].reshape(128, RANK)
-        both = jnp.dot(own, jnp.concatenate(halves(direction), axis=1), preferred_element_type=F32)
+        dir_v[r] = jnp.concatenate(halves(direction), axis=1)
+        both = jnp.dot(own, dir_v[r], preferred_element_type=F32)
         prod_v[r] = both[:, :COLS] + both[:, COLS:]
+
+    def early_rows(r, scale):
+        fac = fac_v[r, :, 0, 0:EARLY, :].reshape(2 * FS * EARLY, RANK)
+        both = jnp.dot(fac, dir_v[r], preferred_element_type=F32)
+        prod = (both[:, :COLS] + both[:, COLS:]).reshape(2 * FS, EARLY, COLS)
+        copy_ref[r, :, 0:EARLY, :] = (early_v[r] - LEARN * (scale * prod)).astype(BF16)
 
     cot_in[0].wait()
 
@@ -304,17 +329,7 @@
         across(r, 1 - core).wait_recv()
         contract(r)
 
-    events = (
-        ((1, facs[0].second), (2, facs[1].second), (3, facs[2].second)),
-        (
-            (0, facs[0].third),
-            (1, facs[1].third),
-            (2, facs[2].third),
-            (2, functools.partial(handed, 0)),
-            (3, functools.partial(handed, 1)),
-        ),
-        ((0, functools.partial(handed, 2)), (1, functools.partial(joined, 0)), (2, functools.partial(joined, 1))),
-    )
+    events = ((1, facs[0].second), (2, facs[1].second), (3, facs[2].second),), ((0, facs[0].third), (1, facs[1].third), (2, facs[2].third), (3, functools.partial(handed, 0)), (3, early_first),), ((0, functools.partial(handed, 1)), (1, functools.partial(handed, 2)), (1, functools.partial(joined, 0)), (2, functools.partial(joined, 1)),)
 
     for r in range(ROLES):
         height = COLS + HEADS if r == 1 else COLS
@@ -323,17 +338,18 @@
         def _(n):
             if r == 0:
                 load(x_hbm.at[:, pl.ds(pl.multiple_of(BLOCK * n, BLOCK), BLOCK)], x_v.at[n], x_sem.at[n]).wait()
-            grad = jnp.dot(lhs_v[r % 2, 0:height, :], x_v[n], preferred_element_type=F32)
             if r + 1 < ROLES:
                 pl.when(n == 0)(cot_in[r + 1].wait)
                 turned(r + 1, n)
+            grad = jnp.dot(lhs_v[r % 2, 0:height, :], x_v[n], preferred_element_type=F32)
             upper, lower = halves(grad[:COLS])
             span = pl.ds(pl.multiple_of(BLOCK * n, BLOCK), BLOCK)
             grad_v[r, 0:COLS, span] = upper
             grad_v[r, COLS:, span] = lower
             if r == 1:
                 for i in range(BLOCK // 128):
-                    gp_v[(BLOCK // 128) * n + i] = grad[COLS:, 128 * i : 128 * i + 128]
+                    for c in (0, 1):
+                        gp_v[(BLOCK // 128) * n + i, c] = grad[COLS + 8 * c : COLS + 8 * c + 8, 128 * i : 128 * i + 128]
             for event, work in events[r]:
                 pl.when(n == event)(work)
 
@@ -352,8 +368,8 @@
             start = start - jnp.where(lane[:, 0:128] == 0, edge, pltpu.roll(start, 1, 1))
             lhs_v[1, COLS:, 0:128] = ((later_v[:, 0:128] + carried) * minus_expm1(start)).astype(BF16)
         if r == 1:
-            to_peers(lambda peer: gp_v.at[peer], grs_v.at[me], 1)
-            grs_v[me] = gp_v[me]
+            to_peers(lambda peer: gp_v.at[peer, core], grs_v.at[me], 1)
+            grs_v[me] = gp_v[me, core]
 
     joined(2)
     for c in rest_in:
@@ -369,16 +385,16 @@
             second = BETA_TWO * sm_v[r, own] + (1.0 - BETA_TWO) * low * low
             direction = first * lax.rsqrt(second)
             squares = squares + direction * direction
-        return squares[:, :128] + squares[:, 128:]
+        return jnp.sum(squares[:, :128] + squares[:, 128:], axis=0, keepdims=True)
 
     from_peers(grs_v, 1)
-    gfull_v[me] = jnp.sum(grs_v[...], axis=0)
+    gfull_v[me, core] = jnp.sum(grs_v[...], axis=0)
     second_sum(0)
     second_sum(1)
+    second_sum(2)
+    early.second(True, (1, 3))
     first_spread(0)
-    second_sum(2)
     first_spread(1)
-    second_spread(0)
     first_spread(2)
 
     ss_v[tp] = slice_squares(0) + slice_squares(1) + slice_squares(2)
@@ -388,12 +404,15 @@
         put(ss_v.at[tp], ss_v.at[tp], ss_sem.at[0], ss_sem.at[1], {"tp": (tp + d) % TP}).start()
 
     squares = put(ss_v.at[pl.ds(0, TP - 1)], ss_v.at[pl.ds(0, TP - 1)], ss_sem.at[0], ss_sem.at[1], {"tp": (tp + 1) % TP})
-    to_peers(lambda peer: gfull_v.at[me], gfull_v.at[me], 2)
+    early.second(False, (2,))
+    to_peers(lambda peer: gfull_v.at[me, core], gfull_v.at[me, core], 2)
+    second_spread(0)
     second_spread(1)
     squares.wait_recv()
     st_v[me] = jnp.sum(ss_v[...], axis=0)
     to_peers(lambda peer: st_v.at[me], st_v.at[me], 3)
     second_spread(2)
+    early.third()
     whole(0, 3).wait_recv()
     finish(0)
     whole(1, 3).wait_recv()
@@ -406,7 +425,11 @@
     scale = lax.rsqrt(total * (1.0 / (ROLES * RANK * COLS * TP)) + 1e-06)
     copies = [
         Gather(
-            me, lambda i, h, r=r: copy_ref.at[r, 2 * i + h], lambda n, r=r: copy_ref.at[r, pl.ds(0, n)], c_send.at[r], c_recv.at[r]
+            me,
+            lambda i, h, r=r: copy_ref.at[r, 2 * i + h, pl.ds(EARLY, 64 - EARLY)],
+            lambda n, r=r: copy_ref.at[r, pl.ds(0, n), pl.ds(EARLY, 64 - EARLY)],
+            c_send.at[r],
+            c_recv.at[r],
         )
         for r in range(ROLES)
     ]
@@ -415,13 +438,15 @@
         new = master_v[r] - LEARN * step
         step_ref[r] = step
         new_ref[r] = new
-        copy_ref[r, pl.ds(2 * me, 2)] = new.astype(BF16).reshape(2, 64, COLS)
+        copy_ref[r, pl.ds(2 * me, 2), EARLY:, :] = new.astype(BF16).reshape(2, 64, COLS)[:, EARLY:, :]
         copies[r].first()
 
-    from_peers(gfull_v, 2)
+    from_peers(grs_v, 2)
+    other_gates(core).start()
+    other_gates(1 - core).wait_recv()
     for i in range(FS):
         cut = slice(128 * i, 128 * i + 128)
-        gate = gfull_v[i]
+        gate = gfull_v[i].reshape(HEADS, 128)
         first = BETA_ONE * gf_v[:, cut] + (1.0 - BETA_ONE) * gate
         second = BETA_TWO * gs_v[:, cut] + (1.0 - BETA_TWO) * gate * gate
         new = gm_v[:, cut] - LEARN * (first * lax.rsqrt(second))
@@ -432,14 +457,19 @@
     squares.wait_send()
     for r in range(ROLES):
         across(r, core).wait_send()
-        for phase in range(4):
-            whole(r, phase).wait_send()
+        put(lowp_v.at[pl.ds(0, 2), pl.ds(0, 240)], lowp_v.at[pl.ds(0, 2), pl.ds(0, 240)], s_send.at[r], s_recv.at[r, 0], {"fs": (me + 1) % FS}).wait_send()
     sent(gx_v, 0)
-    sent(gp_v, 1)
-    sent(gfull_v, 2)
+    sent(grs_v, 1)
+    sent(grs_v, 2)
+    other_gates(core).wait_send()
     sent(st_v, 3)
     for r in range(ROLES):
         facs[r].drain()
+
+    early.last()
+    for r in range(ROLES):
+        early_rows(r, scale)
+    early.drain()
 
     for step in ("second", "third", "last", "drain"):
         for gather in copies:
@@ -492,15 +522,18 @@
             vmem((ROLES, 2, 32, COLS), F32),
             vmem((ROLES, 2, 3, 8, COLS), F32),
             moments,
-            vmem((FS, HEADS, 128), F32),
-            vmem((FS, HEADS, 128), F32),
-            vmem((FS, HEADS, 128), F32),
+            vmem((FS, 2, 8, 128), F32),
+            vmem((FS, 8, 128), F32),
+            vmem((FS, 2, 8, 128), F32),
             vmem((ROLES, 128, COLS), F32),
-            vmem((TP, 8, 128), F32),
-            vmem((FS, 8, 128), F32),
-            dma((10,)), dma((BLOCKS,)), dma((ROLES,)),
-            dma((4,)), dma((4,)), dma((ROLES, 4)), dma((ROLES, 4)), dma((2,)),
-            dma((ROLES,)), dma((ROLES, 15)), dma((ROLES,)), dma((ROLES,)), dma((ROLES,)), dma((ROLES, 15)),
+            vmem((TP, 1, 128), F32),
+            vmem((FS, 1, 128), F32),
+            vmem((ROLES, 2 * FS, EARLY, COLS), F32),
+            vmem((ROLES, RANK, 2 * COLS), BF16),
+            dma((12,)), dma((BLOCKS,)), dma((ROLES,)),
+            dma((4,)), dma((4,)), dma((ROLES,)), dma((ROLES, 4)), dma((2,)),
+            dma((ROLES,)), dma((ROLES, 3)), dma((ROLES + 1,)), dma((ROLES + 1,)), dma((ROLES,)), dma((ROLES, 8)),
+            dma((1,)), dma((8,)),
         ],
         compiler_params=pltpu.CompilerParams(
             collective_id=0, has_side_effects=True, vmem_limit_bytes=57 * 1024 * 1024

time: 71.8 us -> 65.5 us (0.912)
  Pallas kernels: 70.7 us -> 64.8 us
    pallas_call x1, Pallas kernels: 68.1 us -> 62.1 us  [local(): pl.pallas_call(kernel, out_shape=[vmem(s, d) for s, d in shapes], in_spec...]
where the time goes in v3:
time: 65.5 us; the launch traced here: 65.4 us
  Pallas kernels  64.8 us (99%)
    pallas_call x1, Pallas kernels, local(): pl.pallas_call(kernel, out_shape=[vmem(s, d) for s, d in shapes], in_spec...  62.1 us
    pallas_call x1, Pallas kernels, local(): pl.pallas_call(written, out_shape=[jax.ShapeDtypeStruct(s, d) for s, d in...  2.63 us

profile of v3, /device:TPU:0, one launch (start us, length us, event | category | flops | bytes accessed | tf_op | source)
XLA Modules:
  0.0 65.4 jit_solution(6845837814832825813)
XLA Ops:
  0.6 62.1 %shard_map.178 = (f32[3,128,256]{2,1,0:T(8,128)S(1)}, f32[3,128,256]{2,1,0:T(8,128)S(1)}, bf16[3,32,64,256]{3,2,1,0:T(8,128)(2,1)S(1)}, f32[3,256,256]{2,1,0:T(8...) custom-call(bf16[3072,2048]{1,0:T(8,128)(2,1)} %x_hbm.1, ...), custom_call_target="tpu_custom_call" | custom-call | tf_op jit(solution)/shard_map/pallas_call | solution.py:502
  62.8 2.6 %shard_map.179 = (f32[3,128,256]{2,1,0:T(8,128)}, f32[3,128,256]{2,1,0:T(8,128)}, bf16[3,32,64,256]{3,2,1,0:T(8,128)(2,1)}, f32[3,256,256]{2,1,0:T(8,128)}, f32[...) custom-call(f32[3,128,256]{2,1,0:T(8,128)S(1)} %get-tuple-element.27, ...), custom_call_target="tpu_custom_call" | custom-call | tf_op jit(solution)/shard_map/pallas_call | solution.py:542

commit v4 on v3

--- a/solution.py
+++ b/solution.py
@@ -127,6 +127,16 @@
     me, tp = lax.axis_index("fs"), lax.axis_index("tp")
     core = tp % 2
 
+    barrier = pltpu.get_barrier_semaphore()
+
+    @pl.loop(1, FS)
+    def _(d):
+        pl.semaphore_signal(barrier, inc=1, device_id={"fs": (me + d) % FS}, device_id_type=MESH)
+
+    @pl.loop(1, TP)
+    def _(d):
+        pl.semaphore_signal(barrier, inc=1, device_id={"tp": (tp + d) % TP}, device_id_type=MESH)
+
     def load(src, dst, sem):
         return pltpu.make_async_copy(src, dst, sem)
 
@@ -147,16 +157,6 @@
     early_in = [load(master_hbm.at[:, pl.ds(64 * h, EARLY), :], early_v.at[:, 2 * me + h], in_sem.at[10 + h]) for h in (0, 1)]
     for c in (*fac_in, ccot_in, logs_in, cot_in[0], x_in[0], cot_in[1], *x_in[1:], cot_in[2], *early_in, *rest_in):
         c.start()
-
-    barrier = pltpu.get_barrier_semaphore()
-
-    @pl.loop(1, FS)
-    def _(d):
-        pl.semaphore_signal(barrier, inc=1, device_id={"fs": (me + d) % FS}, device_id_type=MESH)
-
-    @pl.loop(1, TP)
-    def _(d):
-        pl.semaphore_signal(barrier, inc=1, device_id={"tp": (tp + d) % TP}, device_id_type=MESH)
 
     def put(src, dst, send, recv, to):
         return pltpu.make_async_remote_copy(src, dst, send, recv, device_id=to, device_id_type=MESH)
@@ -329,7 +329,7 @@
         across(r, 1 - core).wait_recv()
         contract(r)
 
-    events = ((1, facs[0].second), (2, facs[1].second), (3, facs[2].second),), ((0, facs[0].third), (1, facs[1].third), (2, facs[2].third), (3, functools.partial(handed, 0)), (3, early_first),), ((0, functools.partial(handed, 1)), (1, functools.partial(handed, 2)), (1, functools.partial(joined, 0)), (2, functools.partial(joined, 1)),)
+    events = ((1, facs[0].second), (2, facs[1].second), (3, facs[2].second),), ((0, facs[0].third), (1, facs[1].third), (2, facs[2].third), (3, functools.partial(handed, 0)), (3, early_first),), ((0, functools.partial(handed, 1)), (1, functools.partial(handed, 2)), (1, functools.partial(joined, 0)), (2, functools.partial(joined, 1)), (3, functools.partial(joined, 2)),)
 
     for r in range(ROLES):
         height = COLS + HEADS if r == 1 else COLS
@@ -371,7 +371,6 @@
             to_peers(lambda peer: gp_v.at[peer, core], grs_v.at[me], 1)
             grs_v[me] = gp_v[me, core]
 
-    joined(2)
     for c in rest_in:
         c.wait()
 
@@ -392,9 +391,9 @@
     second_sum(0)
     second_sum(1)
     second_sum(2)
-    early.second(True, (1, 3))
     first_spread(0)
     first_spread(1)
+    early.second(True, (1, 3))
     first_spread(2)
 
     ss_v[tp] = slice_squares(0) + slice_squares(1) + slice_squares(2)
@@ -404,19 +403,19 @@
         put(ss_v.at[tp], ss_v.at[tp], ss_sem.at[0], ss_sem.at[1], {"tp": (tp + d) % TP}).start()
 
     squares = put(ss_v.at[pl.ds(0, TP - 1)], ss_v.at[pl.ds(0, TP - 1)], ss_sem.at[0], ss_sem.at[1], {"tp": (tp + 1) % TP})
-    early.second(False, (2,))
-    to_peers(lambda peer: gfull_v.at[me, core], gfull_v.at[me, core], 2)
     second_spread(0)
     second_spread(1)
+    early.second(False, (2,))
     squares.wait_recv()
     st_v[me] = jnp.sum(ss_v[...], axis=0)
     to_peers(lambda peer: st_v.at[me], st_v.at[me], 3)
     second_spread(2)
-    early.third()
+    to_peers(lambda peer: gfull_v.at[me, core], gfull_v.at[me, core], 2)
     whole(0, 3).wait_recv()
     finish(0)
     whole(1, 3).wait_recv()
     finish(1)
+    early.third()
     whole(2, 3).wait_recv()
     finish(2)
 

time: 65.5 us -> 64.2 us (0.980)
  Pallas kernels: 64.8 us -> 63.3 us
    pallas_call x1, Pallas kernels: 62.1 us -> 60.7 us  [local(): pl.pallas_call(kernel, out_shape=[vmem(s, d) for s, d in shapes], in_spec...]
where the time goes in v4:
time: 64.2 us; the launch traced here: 64 us
  Pallas kernels  63.3 us (99%)
  between operations  0.65 us (1%)
    pallas_call x1, Pallas kernels, local(): pl.pallas_call(kernel, out_shape=[vmem(s, d) for s, d in shapes], in_spec...  60.7 us
    pallas_call x1, Pallas kernels, local(): pl.pallas_call(written, out_shape=[jax.ShapeDtypeStruct(s, d) for s, d in...  2.63 us

profile of v4, /device:TPU:0, one launch (start us, length us, event | category | flops | bytes accessed | tf_op | source)
XLA Modules:
  0.0 64.0 jit_solution(587717534504011979)
XLA Ops:
  0.6 60.7 %shard_map.178 = (f32[3,128,256]{2,1,0:T(8,128)S(1)}, f32[3,128,256]{2,1,0:T(8,128)S(1)}, bf16[3,32,64,256]{3,2,1,0:T(8,128)(2,1)S(1)}, f32[3,256,256]{2,1,0:T(8...) custom-call(bf16[3072,2048]{1,0:T(8,128)(2,1)} %x_hbm.1, ...), custom_call_target="tpu_custom_call" | custom-call | tf_op jit(solution)/shard_map/pallas_call | solution.py:501
  61.3 2.6 %shard_map.179 = (f32[3,128,256]{2,1,0:T(8,128)}, f32[3,128,256]{2,1,0:T(8,128)}, bf16[3,32,64,256]{3,2,1,0:T(8,128)(2,1)}, f32[3,256,256]{2,1,0:T(8,128)}, f32[...) custom-call(f32[3,128,256]{2,1,0:T(8,128)S(1)} %get-tuple-element.27, ...), custom_call_target="tpu_custom_call" | custom-call | tf_op jit(solution)/shard_map/pallas_call | solution.py:541

commit v5 on v4

--- a/solution.py
+++ b/solution.py
@@ -231,15 +231,6 @@
         whole(r, 2).wait_recv()
         swap(r, 3)
 
-    ccot_in.wait()
-    logs_in.wait()
-    small = lax.broadcasted_iota(jnp.int32, (8, 128), 1)
-    sums = jnp.sum(ccot_v[...], axis=1, keepdims=True)
-    ends = logs_v[:, TOK - 128 :][:, 127:128]
-    message = jnp.where(small < 32, sums[:8], sums[8:])
-    message = jnp.where(small < 64, message, ends[:8])
-    gx_v[me] = jnp.where(small < 96, message, ends[8:])
-
     facs = [
         Gather(
             me,
@@ -254,8 +245,18 @@
     fac_in[0].wait()
     fac_in[1].wait()
     pl.semaphore_wait(barrier, FS + TP - 2)
+    facs[0].first()
+
+    ccot_in.wait()
+    logs_in.wait()
+    small = lax.broadcasted_iota(jnp.int32, (8, 128), 1)
+    sums = jnp.sum(ccot_v[...], axis=1, keepdims=True)
+    ends = logs_v[:, TOK - 128 :][:, 127:128]
+    message = jnp.where(small < 32, sums[:8], sums[8:])
+    message = jnp.where(small < 64, message, ends[:8])
+    gx_v[me] = jnp.where(small < 96, message, ends[8:])
     to_peers(lambda peer: gx_v.at[me], gx_v.at[me], 0)
-    for r in range(ROLES):
+    for r in range(1, ROLES):
         facs[r].first()
 
     lane = lax.broadcasted_iota(jnp.int32, (HEADS, TOK), 1)

time: 64.2 us -> 64.2 us (level)
  no operation moved by 1% of the time
where the time goes in v5:
time: 64.2 us; the launch traced here: 64.1 us
  Pallas kernels  63.5 us (99%)
  between operations  0.65 us (1%)
    pallas_call x1, Pallas kernels, local(): pl.pallas_call(kernel, out_shape=[vmem(s, d) for s, d in shapes], in_spec...  60.8 us
    pallas_call x1, Pallas kernels, local(): pl.pallas_call(written, out_shape=[jax.ShapeDtypeStruct(s, d) for s, d in...  2.63 us

profile of v5, /device:TPU:0, one launch (start us, length us, event | category | flops | bytes accessed | tf_op | source)
XLA Modules:
  0.0 64.1 jit_solution(14685708153081699314)
XLA Ops:
  0.6 60.8 %shard_map.178 = (f32[3,128,256]{2,1,0:T(8,128)S(1)}, f32[3,128,256]{2,1,0:T(8,128)S(1)}, bf16[3,32,64,256]{3,2,1,0:T(8,128)(2,1)S(1)}, f32[3,256,256]{2,1,0:T(8...) custom-call(bf16[3072,2048]{1,0:T(8,128)(2,1)} %x_hbm.1, ...), custom_call_target="tpu_custom_call" | custom-call | tf_op jit(solution)/shard_map/pallas_call | solution.py:502
  61.5 2.6 %shard_map.179 = (f32[3,128,256]{2,1,0:T(8,128)}, f32[3,128,256]{2,1,0:T(8,128)}, bf16[3,32,64,256]{3,2,1,0:T(8,128)(2,1)}, f32[3,256,256]{2,1,0:T(8,128)}, f32[...) custom-call(f32[3,128,256]{2,1,0:T(8,128)S(1)} %get-tuple-element.27, ...), custom_call_target="tpu_custom_call" | custom-call | tf_op jit(solution)/shard_map/pallas_call | solution.py:542
